TPU v7x, 512 devices: a whole 4x8x8 slice. The times are simulated.
512 devices in a mesh: sp: 256 (over z, y, x), tp: 2 (over core).
Axes of the slice: x: 4, y: 8, z: 8, core: 2. Of those that a mesh axis runs over, the one named last changes fastest.
Arguments:
- features: bfloat16 [65536, 1024], P('sp', 'tp'), may hold values from -6 to 6
- lambda_real: float32 [64, 64], P('tp'), may hold values from -4 to 0, as said below
- lambda_imag: float32 [64, 64], P('tp'), may hold values from 0.5 to 201.06177
- log_step: float32 [64], P('tp'), may hold values from -5 to -2
- input_real: float32 [64, 64, 16], P('tp'), may hold values from -0.5 to 0.5
- input_imag: float32 [64, 64, 16], P('tp'), may hold values from -0.5 to 0.5
- real_output: float32 [64, 16, 64], P('tp'), may hold values from -0.75 to 0.75
- imaginary_output: float32 [64, 16, 64], P('tp'), may hold values from -0.75 to 0.75
- skip_gain: float32 [1024], P('tp'), may hold values from -4 to 4
- value_weight: bfloat16 [1024, 2048], P('tp'), may hold values from -0.1875 to 0.1875
- gate_weight: bfloat16 [1024, 2048], P('tp'), may hold values from -0.1875 to 0.1875
- value_bias: float32 [2048], replicated, may hold values from -3 to 3
- gate_bias: float32 [2048], replicated, may hold values from -3 to 3
Outputs:
- mixed_output: bfloat16 [65536, 2048], P(('sp', 'tp'))
Inputs may be any that keep to these rules, and one draw needn't show every extreme that they name: `lambda_real`: negative.
All inputs are finite; a program needn't handle non-finite values.
Results may differ from a plain program's by a relative error of at most 0.03.
Values may be sent and summed in bfloat16 or wider, within the bound.
No kernel may reach another device: no remote copies, remote signals or barrier semaphores. Data moves between devices by JAX's collectives and lax.ppermute only.
A program may use at most 128 MiB of HBM per device.

v0:
```python
import math

import jax
import jax.numpy as jnp
from jax import lax
from jax.sharding import Mesh
from jax.sharding import PartitionSpec as P

SP = ("sp_0", "sp_1", "sp_2")
SP_TP = ("sp_0", "sp_1", "sp_2", "tp")


def filled_with(shard, identity):
    return jax.tree.map(
        lambda a, e: jnp.broadcast_to(jnp.asarray(e, a.dtype), a.shape), shard, identity
    )


def gathered_once(shard, axis):
    leaves = jax.tree.leaves(shard)
    sequence = sorted(range(len(leaves)), key=lambda k: -leaves[k].size)
    width = (1, *leaves[sequence[0]].shape)[-1]
    lines = [
        jnp.pad(leaves[k].reshape(-1), (0, -leaves[k].size % width)).reshape(-1, width)
        for k in sequence
    ]
    both, at, found = (lax.all_gather(jnp.concatenate(lines), axis), 0, {})
    for k, line in zip(sequence, lines):
        share = both[:, at : at + len(line)].reshape(len(both), -1)
        found[k] = share[:, : leaves[k].size].reshape(-1, *leaves[k].shape)
        at += len(line)
    numbers = iter(range(len(leaves)))
    return jax.tree.map(lambda _: found[next(numbers)], shard)


def prefix_by_axis(shard, axes, combine, identity):
    before = start = filled_with(shard, identity)
    total = shard
    for axis in reversed(axes):
        devices, index = (lax.axis_size(axis), lax.axis_index(axis))
        pieces = gathered_once(total, axis)
        inside, total = (start, start)
        for k in range(devices):
            passed = k < index
            total = combine(total, jax.tree.map(lambda part: part[k], pieces))
            inside = jax.tree.map(lambda new, old: jnp.where(passed, new, old), total, inside)
        before = combine(inside, before)
    return before


def in_one_piece(arrays, axis, dim, along):
    widths = [a.shape[along] for a in arrays]
    both = jnp.concatenate(arrays, axis=along)
    out = lax.all_gather(both, axis, axis=dim, tiled=True)
    return tuple(jnp.split(out, [sum(widths[:k]) for k in range(1, len(widths))], axis=along))


def discretize(lambda_real, lambda_imag, log_step, input_real, input_imag):
    step_size = jnp.exp(log_step)[:, None]
    magnitude = jnp.exp(lambda_real * step_size)
    phase_arg = lambda_imag * step_size
    trans_re = magnitude * jnp.cos(phase_arg)
    trans_im = magnitude * jnp.sin(phase_arg)
    denominator = lambda_real * lambda_real + lambda_imag * lambda_imag
    num_re = trans_re - 1.0
    f_re = (num_re * lambda_real + trans_im * lambda_imag) / denominator
    f_im = (trans_im * lambda_real - num_re * lambda_imag) / denominator
    bar_re = f_re[..., None] * input_real - f_im[..., None] * input_imag
    bar_im = f_re[..., None] * input_imag + f_im[..., None] * input_real
    return (step_size, bar_re, bar_im)


def powers_flat(lambda_real, lambda_imag, step_size, first, count):
    exponent = (jnp.arange(count, dtype=jnp.int32) + first).astype(jnp.float32)[:, None]
    rate_re = (lambda_real * step_size).reshape(1, -1)
    rate_im = (lambda_imag * step_size).reshape(1, -1)
    magnitude = jnp.exp(exponent * rate_re)
    phase_arg = exponent * rate_im
    return (magnitude * jnp.cos(phase_arg), magnitude * jnp.sin(phase_arg))


def combine(earlier, later):
    a1r, a1i, b1r, b1i = earlier
    a2r, a2i, b2r, b2i = later
    return (
        a1r * a2r - a1i * a2i,
        a1r * a2i + a1i * a2r,
        a2r * b1r - a2i * b1i + b2r,
        a2r * b1i + a2i * b1r + b2i,
    )


def within_blocks(step_re, step_im, bu_re, bu_im, span):
    blocks_re = bu_re.reshape(-1, span, bu_re.shape[1])
    blocks_im = bu_im.reshape(-1, span, bu_im.shape[1])
    h_re = jnp.zeros_like(blocks_re[:, 0])
    h_im = jnp.zeros_like(blocks_im[:, 0])
    rows_re = []
    rows_im = []
    for offset in range(span):
        new_re = step_re * h_re - step_im * h_im + blocks_re[:, offset]
        new_im = step_re * h_im + step_im * h_re + blocks_im[:, offset]
        h_re, h_im = (new_re, new_im)
        rows_re.append(h_re)
        rows_im.append(h_im)
    return (jnp.stack(rows_re, axis=1), jnp.stack(rows_im, axis=1))


def block_carries(span_re, span_im, ends_re, ends_im, start_re, start_im):

    def advance(carried, ends):
        c_re, c_im = carried
        e_re, e_im = ends
        next_re = span_re * c_re - span_im * c_im + e_re
        next_im = span_re * c_im + span_im * c_re + e_im
        return ((next_re, next_im), (c_re, c_im))

    final, entering = lax.scan(advance, (start_re, start_im), (ends_re, ends_im))
    return (final, entering)


def local(
    features,
    lambda_real,
    lambda_imag,
    log_step,
    input_real,
    input_imag,
    real_output,
    imaginary_output,
    skip_gain,
    value_weight,
    gate_weight,
    value_bias,
    gate_bias,
):
    positions = features.shape[0]
    groups = lambda_real.shape[0]
    state_width = lambda_real.shape[1]
    group_size = input_real.shape[2]
    flat_width = groups * state_width
    span = math.gcd(positions, 16)
    step_size, bar_re, bar_im = discretize(
        lambda_real, lambda_imag, log_step, input_real, input_imag
    )
    inner_re, inner_im = powers_flat(lambda_real, lambda_imag, step_size, 1, span)
    whole_re, whole_im = powers_flat(lambda_real, lambda_imag, step_size, positions, 1)
    step_re, step_im = (inner_re[0], inner_im[0])
    span_re, span_im = (inner_re[-1], inner_im[-1])
    widened = features.astype(jnp.float32)
    grouped = widened.reshape(positions, groups, group_size)
    bu_re = jnp.einsum("sgc,gpc->sgp", grouped, bar_re).reshape(positions, flat_width)
    bu_im = jnp.einsum("sgc,gpc->sgp", grouped, bar_im).reshape(positions, flat_width)
    local_re, local_im = within_blocks(step_re, step_im, bu_re, bu_im, span)
    ends_re, ends_im = (local_re[:, -1], local_im[:, -1])
    zero_state = jnp.zeros((flat_width,), jnp.float32)
    ones_state = jnp.ones((flat_width,), jnp.float32)
    identity = (ones_state, zero_state, zero_state, zero_state)
    final, unused = block_carries(span_re, span_im, ends_re, ends_im, zero_state, zero_state)
    incoming = prefix_by_axis((whole_re[0], whole_im[0], final[0], final[1]), SP, combine, identity)
    h_re, h_im = (incoming[2], incoming[3])
    later, entering = block_carries(span_re, span_im, ends_re, ends_im, h_re, h_im)
    enter_re = entering[0][:, None]
    enter_im = entering[1][:, None]
    signal_real = (local_re + inner_re * enter_re - inner_im * enter_im).reshape(
        positions, flat_width
    )
    signal_imaginary = (local_im + inner_re * enter_im + inner_im * enter_re).reshape(
        positions, flat_width
    )
    signal_real = signal_real.reshape(positions, groups, state_width)
    signal_imaginary = signal_imaginary.reshape(positions, groups, state_width)
    mixer_response = jnp.einsum("qej,eoj->qeo", signal_real, real_output) - jnp.einsum(
        "qej,eoj->qeo", signal_imaginary, imaginary_output
    )
    mixer_response = mixer_response.reshape(positions, groups * group_size) + skip_gain * widened
    activated = jax.nn.gelu(mixer_response).astype(jnp.bfloat16)
    model_width = value_weight.shape[1]
    moved = lax.all_to_all(activated, "tp", split_axis=0, concat_axis=1, tiled=True)
    full_value, full_gate = in_one_piece((value_weight, gate_weight), "tp", 0, 1)
    pieces = lax.axis_size("tp")
    row_total = moved.shape[0]
    slice_width = value_weight.shape[0]
    blocks_act = moved.reshape(row_total, pieces, slice_width)

    def halves(weight):
        partial_value = jnp.einsum(
            "rnc,ncd->nrd",
            blocks_act,
            weight.reshape(pieces, slice_width, model_width),
            preferred_element_type=jnp.float32,
        )
        rounded = lax.optimization_barrier(partial_value.astype(jnp.bfloat16))
        return jnp.sum(rounded.astype(jnp.float32), axis=0)

    value_sum = halves(full_value)
    gate_sum = halves(full_gate)
    value_sum = value_sum + value_bias
    gate_sum = gate_sum + gate_bias
    return (value_sum * jax.nn.sigmoid(gate_sum)).astype(jnp.bfloat16)


def solution(mesh):
    split = Mesh(mesh.devices.reshape(8, 8, 4, mesh.shape["tp"]), ("sp_0", "sp_1", "sp_2", "tp"))
    in_specs = (
        P(SP, "tp"),
        P("tp", None),
        P("tp", None),
        P("tp"),
        P("tp", None, None),
        P("tp", None, None),
        P("tp", None, None),
        P("tp", None, None),
        P("tp"),
        P("tp", None),
        P("tp", None),
        P(),
        P(),
    )
    out_specs = P(SP_TP, None)
    return jax.shard_map(local, mesh=split, in_specs=in_specs, out_specs=out_specs, check_vma=False)
```

profile of v0, /device:TPU:1, one launch (start us, length us, event | category | flops | bytes accessed | tf_op | source)
XLA Modules:
  0.0 200.4 jit_solution(3189356863215950880)
XLA Ops:
  6.5 4.8 %pad_maximum_fusion = bf16[512,4096]{1,0:T(8,128)(2,1)} fusion(bf16[512,2048]{1,0:T(8,128)(2,1)} %param.27, bf16[512,2048]{1,0:T(8,128)(2,1)} %param.26), kind=kLoop, calls=%fused_computation.8 | loop fusion | flops 8388608 | bytes 8388608 | tf_op jit(solution)/shard_map/concatenate | solution.py:53
  13.2 1.8 convolution_bitcast_fusion.1
  16.5 5.5 %copy.90 = f32[256,32,64]{2,1,0:T(8,128)} copy(f32[256,32,64]{0,2,1:T(8,128)} %convolution_bitcast_fusion.1) | data formatting | bytes 4194304 | tf_op jit(solution)/shard_map/sgc,gpc->sgp/transpose | solution.py:152
  22.0 5.0 %reshape_reshape.8 = f32[16,16,2048]{2,1,0:T(8,128)} reshape(f32[256,32,64]{2,1,0:T(8,128)} %copy.90) | data formatting | bytes 4194304 | tf_op jit(solution)/shard_map/reshape;reshape | solution.py:94
  27.0 10.1 %fusion.82 = (f32[16,1,2048]{2,1,0:T(1,128)}, f32[16,1,2048]{2,1,0:T(1,128)S(1)}, f32[16,1,2048]{2,1,0:T(1,128)}, f32[16,1,2048]{2,1,0:T(1,128)}, f32[16,1,2048]...) fusion(f32[16,16,2048]{2,1,0:T(8,128)} %reshape_reshape.8), kind=kLoop, calls=%fused_computation.399 | loop fusion | bytes 4194304 | tf_op jit(solution)/shard_map/slice | solution.py:101
  37.1 4.5 %copy.92 = f32[256,32,64]{2,1,0:T(8,128)} copy(f32[256,32,64]{0,2,1:T(8,128)S(1)} %convolution_bitcast_fusion) | data formatting | bytes 4194304 | tf_op jit(solution)/shard_map/sgc,gpc->sgp/transpose | solution.py:153
  41.6 3.6 %reshape_reshape.9 = f32[16,16,2048]{2,1,0:T(8,128)S(1)} reshape(f32[256,32,64]{2,1,0:T(8,128)} %copy.92) | data formatting | bytes 4194304 | tf_op jit(solution)/shard_map/reshape;reshape | solution.py:95
  45.3 1.6 fusion.81
  50.7 1.0 while.30
  51.8 10.4 %all-gather.3 = f32[4,4,2048]{2,1,0:T(4,128)S(1)} all-gather(f32[1,4,2048]{2,1,0:T(4,128)S(1)} %maximum_bitcast_fusion), channel_id=2, replica_groups=mesh['sp_0'=8,'sp_1'=8,'sp_2'=4,'tp'=2] {'sp_2'}, dimensions={0}, use_global_device_ids=true | all-gather | bytes 163840 | tf_op jit(solution)/shard_map/all_gather | solution.py:27
  62.6 21.2 %all-gather.4 = f32[8,4,2048]{2,1,0:T(4,128)S(1)} all-gather(f32[1,4,2048]{2,1,0:T(4,128)S(1)} %maximum_bitcast_fusion.1), channel_id=3, replica_groups=mesh['sp_0'=8,'sp_1'=8,'sp_2'=4,'tp'=2] {'sp_1'}, dimensions={0}, use_global_device_ids=true | all-gather | bytes 294912 | tf_op jit(solution)/shard_map/all_gather | solution.py:27
  85.4 26.2 %all-gather.5 = f32[8,4,2048]{2,1,0:T(4,128)S(1)} all-gather(f32[1,4,2048]{2,1,0:T(4,128)S(1)} %maximum_bitcast_fusion.2), channel_id=4, replica_groups=mesh['sp_0'=8,'sp_1'=8,'sp_2'=4,'tp'=2] {'sp_0'}, dimensions={0}, use_global_device_ids=true | all-gather | bytes 294912 | tf_op jit(solution)/shard_map/all_gather | solution.py:27
  122.8 1.3 copy-done.3
  124.5 21.6 %while.29 = (s32[]{:T(128)}, f32[2048]{0:T(1024)S(1)}, f32[2048]{0:T(1024)S(1)}, f32[16,2048]{1,0:T(8,128)S(1)}, f32[16,2048]{1,0:T(8,128)S(1)}, /*index=5*/f32[...) while((s32[]{:T(128)}, f32[2048]{0:T(1024)S(1)}, ...), condition=%wide.region_3.4_spmd, body=%wide.region_2.3_spmd.sunk | while | flops 16386 | bytes 131201 | solution.py:118
  146.1 3.3 %multiply_subtract_fusion = (bf16[16,16,2048]{2,0,1:T(8,128)(2,1)S(1)}, bf16[16,16,2048]{2,0,1:T(8,128)(2,1)}) fusion(f32[16,16,2048]{2,0,1:T(8,128)S(1)} %copy-done.2, f32[16,2048]{1,0:T(8,128)S(1)} %get-tuple-element.94, f32[16,2048]{1,0:T(8,128)S(1)} %copy-done.52, f32[16,2048]{1,0:T(8,128)S(1)} %get-tuple-element.93, f32[16,2048]{1,0:T(8,128)S(1)} %copy-done.50, ...), kind=kLoop, calls=%fused_computation.18 | loop fusion | flops 5242880 | bytes 6815744 | tf_op jit(solution)/shard_map/sub | solution.py:165
  150.0 2.2 %sub.837 = bf16[256,32,64]{2,1,0:T(8,128)(2,1)S(1)} reshape(bf16[16,16,2048]{2,1,0:T(8,128)(2,1)S(1)} %copy.124) | data formatting | bytes 2097152 | tf_op jit(solution)/shard_map/sub | solution.py:165
  152.2 1.8 copy.126
  154.0 3.2 %add.2136 = bf16[256,32,64]{2,1,0:T(8,128)(2,1)} reshape(bf16[16,16,2048]{2,1,0:T(8,128)(2,1)S(1)} %copy.126) | data formatting | bytes 2097152 | tf_op jit(solution)/shard_map/add | solution.py:168
  157.2 2.7 %fusion = f32[32,256,16]{1,2,0:T(8,128)S(1)} fusion(f32[32,16,64]{2,1,0:T(8,128)S(1)} %copy-done, bf16[256,32,64]{2,1,0:T(8,128)(2,1)} %add.2136), kind=kOutput, calls=%fused_computation.9 | convolution fusion | flops 16777216 | bytes 1703936 | tf_op jit(solution)/shard_map/qej,eoj->qeo/dot_general | solution.py:173
  159.9 1.0 fusion.4
  162.1 19.3 %all-to-all-start = ((bf16[2,128,512]{2,1,0:T(8,128)(2,1)}), bf16[2,128,512]{2,1,0:T(8,128)(2,1)S(1)}, u32[]{:S(2)}, u32[]{:S(2)}) async-start(bf16[2,128,512]{2,1,0:T(8,128)(2,1)} %bitcast.161), calls=%async_computation | async-start | bytes 524288 | tf_op jit(solution)/shard_map/all_to_all | solution.py:179
  181.4 6.1 %fusion.80 = (bf16[1024,2048]{1,0:T(8,128)(2,1)}, bf16[1024,2048]{1,0:T(8,128)(2,1)}) fusion(bf16[1024,4096]{1,0:T(8,128)(2,1)} %all-gather.8.cloned.1.call-done), kind=kLoop, calls=%fused_computation.397 | loop fusion | bytes 16777216 | tf_op jit(solution)/shard_map/split | solution.py:55
  187.5 3.1 %convolution_convert_fusion.1 = bf16[2,128,2048]{2,1,0:T(8,128)(2,1)S(1)} fusion(bf16[2,512,2048]{2,1,0:T(8,128)(2,1)} %bitcast.791, bf16[2,128,512]{2,1,0:T(8,128)(2,1)S(1)} %all-to-all-done), kind=kOutput, calls=%fused_computation.14 | convolution fusion | flops 537395200 | bytes 5505024 | tf_op jit(solution)/shard_map/rnc,ncd->nrd/dot_general | solution.py:187
  192.5 1.1 multiply_convert_fusion
  (309 shorter events, 44.9 us)
Async XLA Ops:
  6.5 150.7 %copy-start = (f32[32,16,64]{2,1,0:T(8,128)S(1)}, f32[32,16,64]{2,1,0:T(8,128)}, u32[]{:S(2)}) copy-start(f32[32,16,64]{2,1,0:T(8,128)} %param.24) | copy-start | bytes 393220
  6.5 174.9 %all-gather.8.cloned.1.call-start = ((), (), s32[]{:S(2)}) async-start(), calls=%async_computation.1 | async-start | bytes 12582912 | tf_op jit(solution)/shard_map/all_gather | solution.py:54
  45.2 3.1 %copy-start.33 = (f32[16,1,2048]{2,1,0:T(1,128)S(1)}, f32[16,1,2048]{2,1,0:T(1,128)}, u32[]{:S(2)}) copy-start(f32[16,1,2048]{2,1,0:T(1,128)} %get-tuple-element.287) | copy-start | bytes 393220
  45.2 3.1 %copy-start.37 = (f32[16,1,2048]{2,1,0:T(1,128)S(1)}, f32[16,1,2048]{2,1,0:T(1,128)}, u32[]{:S(2)}) copy-start(f32[16,1,2048]{2,1,0:T(1,128)} %get-tuple-element.288) | copy-start | bytes 393220
  45.2 3.1 %copy-start.43 = (f32[16,1,2048]{2,1,0:T(1,128)S(1)}, f32[16,1,2048]{2,1,0:T(1,128)}, u32[]{:S(2)}) copy-start(f32[16,1,2048]{2,1,0:T(1,128)} %get-tuple-element.289) | copy-start | bytes 393220
  45.2 3.5 %copy-start.18 = (f32[16,1,2048]{2,1,0:T(1,128)S(1)}, f32[16,1,2048]{2,1,0:T(1,128)}, u32[]{:S(2)}) copy-start(f32[16,1,2048]{2,1,0:T(1,128)} %get-tuple-element.283) | copy-start | bytes 393220
  45.2 3.5 %copy-start.22 = (f32[16,1,2048]{2,1,0:T(1,128)S(1)}, f32[16,1,2048]{2,1,0:T(1,128)}, u32[]{:S(2)}) copy-start(f32[16,1,2048]{2,1,0:T(1,128)} %get-tuple-element.285) | copy-start | bytes 393220
  45.3 3.5 %copy-start.26 = (f32[16,1,2048]{2,1,0:T(1,128)S(1)}, f32[16,1,2048]{2,1,0:T(1,128)}, u32[]{:S(2)}) copy-start(f32[16,1,2048]{2,1,0:T(1,128)} %get-tuple-element.286) | copy-start | bytes 393220
  50.5 33.6 %copy-start.44 = (f32[16,1,2048]{2,1,0:T(1,128)S(1)}, f32[16,1,2048]{2,1,0:T(1,128)}, u32[]{:S(2)}) copy-start(f32[16,1,2048]{2,1,0:T(1,128)} %get-tuple-element.289) | copy-start | bytes 393220
  51.7 10.9 %copy-start.53 = (f32[16,2048]{1,0:T(8,128)}, f32[16,2048]{1,0:T(8,128)S(1)}, u32[]{:S(2)}) copy-start(f32[16,2048]{1,0:T(8,128)S(1)} %get-tuple-element.583) | copy-start | bytes 393220
  51.7 32.4 %copy-start.54 = (f32[16,2048]{1,0:T(8,128)}, f32[16,2048]{1,0:T(8,128)S(1)}, u32[]{:S(2)}) copy-start(f32[16,2048]{1,0:T(8,128)S(1)} %get-tuple-element.584) | copy-start | bytes 393220
  51.7 60.1 %copy-start.38 = (f32[16,1,2048]{2,1,0:T(1,128)S(1)}, f32[16,1,2048]{2,1,0:T(1,128)}, u32[]{:S(2)}) copy-start(f32[16,1,2048]{2,1,0:T(1,128)} %get-tuple-element.288) | copy-start | bytes 393220
  51.7 60.1 %copy-start.42 = (f32[16,1,2048]{2,1,0:T(1,128)S(1)}, f32[16,1,2048]{2,1,0:T(1,128)}, u32[]{:S(2)}) copy-start(f32[16,1,2048]{2,1,0:T(1,128)} %copy-done.41) | copy-start | bytes 393220
  62.6 50.0 %copy-start.34 = (f32[16,1,2048]{2,1,0:T(1,128)S(1)}, f32[16,1,2048]{2,1,0:T(1,128)}, u32[]{:S(2)}) copy-start(f32[16,1,2048]{2,1,0:T(1,128)} %get-tuple-element.287) | copy-start | bytes 393220
  62.6 50.0 %copy-start.40 = (f32[16,1,2048]{2,1,0:T(1,128)S(1)}, f32[16,1,2048]{2,1,0:T(1,128)}, u32[]{:S(2)}) copy-start(f32[16,1,2048]{2,1,0:T(1,128)} %copy-done.39) | copy-start | bytes 393220
  84.9 28.5 %copy-start.27 = (f32[16,1,2048]{2,1,0:T(1,128)S(1)}, f32[16,1,2048]{2,1,0:T(1,128)}, u32[]{:S(2)}) copy-start(f32[16,1,2048]{2,1,0:T(1,128)} %get-tuple-element.286) | copy-start | bytes 393220
  84.9 28.5 %copy-start.36 = (f32[16,1,2048]{2,1,0:T(1,128)S(1)}, f32[16,1,2048]{2,1,0:T(1,128)}, u32[]{:S(2)}) copy-start(f32[16,1,2048]{2,1,0:T(1,128)} %copy-done.35) | copy-start | bytes 393220
  85.4 28.8 %copy-start.23 = (f32[16,1,2048]{2,1,0:T(1,128)S(1)}, f32[16,1,2048]{2,1,0:T(1,128)}, u32[]{:S(2)}) copy-start(f32[16,1,2048]{2,1,0:T(1,128)} %get-tuple-element.285) | copy-start | bytes 393220
  85.4 28.8 %copy-start.29 = (f32[16,1,2048]{2,1,0:T(1,128)S(1)}, f32[16,1,2048]{2,1,0:T(1,128)}, u32[]{:S(2)}) copy-start(f32[16,1,2048]{2,1,0:T(1,128)} %copy-done.28) | copy-start | bytes 393220
  121.9 24.2 %copy-start.50 = (f32[16,2048]{1,0:T(8,128)S(1)}, f32[16,2048]{1,0:T(8,128)}, u32[]{:S(2)}) copy-start(f32[16,2048]{1,0:T(8,128)} %copy-done.49) | copy-start | bytes 393220
  121.9 24.2 %copy-start.52 = (f32[16,2048]{1,0:T(8,128)S(1)}, f32[16,2048]{1,0:T(8,128)}, u32[]{:S(2)}) copy-start(f32[16,2048]{1,0:T(8,128)} %copy-done.51) | copy-start | bytes 393220
  122.7 23.4 %copy-start.2 = (f32[16,16,2048]{2,0,1:T(8,128)S(1)}, f32[16,16,2048]{2,0,1:T(8,128)}, u32[]{:S(2)}) copy-start(f32[16,16,2048]{2,0,1:T(8,128)} %get-tuple-element.151) | copy-start | bytes 6291460
  162.1 25.5 %all-to-all-start = ((bf16[2,128,512]{2,1,0:T(8,128)(2,1)}), bf16[2,128,512]{2,1,0:T(8,128)(2,1)S(1)}, u32[]{:S(2)}, u32[]{:S(2)}) async-start(bf16[2,128,512]{2,1,0:T(8,128)(2,1)} %bitcast.161), calls=%async_computation | async-start | bytes 524288 | tf_op jit(solution)/shard_map/all_to_all | solution.py:179
  187.5 3.5 %copy-start.1 = (bf16[1024,2048]{1,0:T(8,128)(2,1)S(1)}, bf16[1024,2048]{1,0:T(8,128)(2,1)}, u32[]{:S(2)}) copy-start(bf16[1024,2048]{1,0:T(8,128)(2,1)} %get-tuple-element.259) | copy-start | bytes 12582916
  (47 other events, 94.9 us)
Sparse Core Ops, SparseCore 0:
  11.5 34.9 all-gather.7
where the time goes:
time: 202 us; the launch traced here: 200 us
  local copies, waits for them, and re-layouts  70.1 us (35%)
  blocking collectives  57.8 us (29%)
  other arithmetic  27.7 us (14%)
  starting transfers between devices  19.3 us (10%)
  between operations  14.5 us (7%)
  matrix products  9.82 us (5%)
    all_gather x3, blocking collectives, gathered_once(): both, at, found = (lax.all_gather(jnp.concatenate(lines), axis), 0, {})  57.8 us
    all_to_all x1, starting transfers between devices, local(): lax.all_to_all(activated, 'tp', split_axis=0, concat_axis=1, tiled=True)  19.3 us
    dynamic_slice x32, local copies, waits for them, and re-layouts, block_carries(): lax.scan(advance, (start_re, start_im), (ends_re, ends_im))  14.6 us
    unnamed x20, other arithmetic  11.6 us
    slice x1, local copies, waits for them, and re-layouts, within_blocks(): new_re = step_re * h_re - step_im * h_im + blocks_re[:, offset]  10.1 us
    dynamic_update_slice x32, local copies, waits for them, and re-layouts, block_carries(): lax.scan(advance, (start_re, start_im), (ends_re, ends_im))  6.55 us
    split x1, local copies, waits for them, and re-layouts, in_one_piece(): jnp.split(out, [sum(widths[:k]) for k in range(1, len(widths))], axis=along)  6.14 us
    transpose x1, local copies, waits for them, and re-layouts, local(): jnp.einsum('sgc,gpc->sgp', grouped, bar_re).reshape(positions, flat_width)  5.55 us
  transfers between devices with their start and end apart: 2, of which 0 were waited for; matrix products, arithmetic and copies ran while one was open for 47% of the time, Pallas kernels for 0%

commit v1 on v0

v1 whole, which is shorter than its diff:
```python
import functools

import jax
import jax.numpy as jnp
from jax import lax
from jax.experimental import pallas as pl
from jax.experimental.pallas import tpu as pltpu
from jax.sharding import Mesh
from jax.sharding import PartitionSpec as P

SP = ("z", "y", "x")
SP_TP = ("z", "y", "x", "tp")
NEAR = ("y", "x")
FAR = "z"

T = 256
BLOCKS = 8
STEPS = 32
G = 32
STATE = 64
GROUP = 16
CH = 512
FLAT = 2048
LB = 16
HALF = 1024
Q = 4

F32 = jnp.float32
BF16 = jnp.bfloat16
VMEM = pltpu.VMEM


def cmul(ar, ai, br, bi):
    return ar * br - ai * bi, ar * bi + ai * br


def power_rows(a_ref, lo, n):
    return jnp.concatenate(
        [jnp.broadcast_to(a_ref[pl.ds(lo + k, 1), :], (BLOCKS, 128)) for k in range(n)], axis=1
    )


def transition(lr_ref, li_ref, ls_ref):
    row = lax.broadcasted_iota(jnp.int32, (G, STATE), 0)
    logs = jnp.zeros((G, STATE), F32)
    for g in range(G):
        logs = jnp.where(row == g, ls_ref[g], logs)
    step = jnp.exp(logs)
    lr = lr_ref[...]
    li = li_ref[...]
    magnitude = jnp.exp(lr * step)
    phase = li * step
    return lr, li, magnitude * jnp.cos(phase), magnitude * jnp.sin(phase)


def order_matrix(transposed):
    r = lax.broadcasted_iota(jnp.int32, (T, T), 1 if transposed else 0)
    t = lax.broadcasted_iota(jnp.int32, (T, T), 0 if transposed else 1)
    hit = t == (r & 7) * STEPS + (r >> 3)
    return jnp.where(hit, 1.0, 0.0).astype(BF16)


def fold_groups(a):
    row = lax.broadcasted_iota(jnp.int32, (LB, G), 0)
    col = lax.broadcasted_iota(jnp.int32, (LB, G), 1)
    even = jnp.where(col == 2 * row, 1.0, 0.0)
    odd = jnp.where(col == 2 * row + 1, 1.0, 0.0)
    hi = lax.Precision.HIGHEST
    left = jnp.dot(even, a, precision=hi, preferred_element_type=F32)
    right = jnp.dot(odd, a, precision=hi, preferred_element_type=F32)
    return jnp.concatenate([left, right], axis=1)


def first_kernel(
    u_ref, lr_ref, li_ref, ls_ref, br_ref, bi_ref,
    copies_ref, whole_ref, ent_ref, up_ref, xr_ref, xi_ref, a_ref, f_ref,
    fin_ref, pw_ref,
):
    lr, li, ar, ai = transition(lr_ref, li_ref, ls_ref)
    den = lr * lr + li * li
    num = ar - 1.0
    f_ref[0] = (num * lr + ai * li) / den
    f_ref[1] = (ai * lr - num * li) / den

    pr, pi = fold_groups(ar), fold_groups(ai)
    a_ref[0], a_ref[1] = pr, pi
    for _ in range(5):
        pr, pi = cmul(pr, pi, pr, pi)
    for k in range(3):
        pw_ref[2 * k], pw_ref[2 * k + 1] = pr, pi
        a_ref[2 + 2 * k], a_ref[3 + 2 * k] = pr, pi
        pr, pi = cmul(pr, pi, pr, pi)
    whole_ref[0], whole_ref[1] = pr, pi

    up = jnp.dot(order_matrix(False), u_ref[...], preferred_element_type=F32).astype(BF16)
    up_ref[...] = up

    c = lax.broadcasted_iota(jnp.int32, (GROUP, 128), 0)
    lane = lax.broadcasted_iota(jnp.int32, (GROUP, 128), 1)
    spread = jnp.where((lane & 15) == c, 1.0, 0.0).astype(BF16)
    own = (lax.broadcasted_iota(jnp.int32, (512, 128), 0) >> 6) == (
        lax.broadcasted_iota(jnp.int32, (512, 128), 1) >> 4
    )
    for q in range(Q):
        for b_ref, x_ref in ((br_ref, xr_ref), (bi_ref, xi_ref)):
            b = b_ref[pl.ds(512 * q, 512), :].astype(BF16)
            wide = jnp.dot(b, spread, preferred_element_type=F32)
            wide = jnp.where(own, wide, 0.0).astype(BF16)
            x_ref[:, pl.ds(512 * q, 512)] = lax.dot_general(
                up[:, 128 * q : 128 * (q + 1)], wide, (((1,), (1,)), ((), ())),
                preferred_element_type=F32,
            )

    sub = lax.broadcasted_iota(jnp.int32, (BLOCKS, HALF), 0)
    for h in range(2):
        mr = power_rows(a_ref.at[0], 8 * h, 8)
        mi = power_rows(a_ref.at[1], 8 * h, 8)

        def body(j, carried):
            hr, hi = carried
            rows = pl.ds(pl.multiple_of(j * BLOCKS, BLOCKS), BLOCKS)
            nr, ni = cmul(mr, mi, hr, hi)
            nr = nr + xr_ref[rows, pl.ds(HALF * h, HALF)]
            ni = ni + xi_ref[rows, pl.ds(HALF * h, HALF)]
            return nr, ni

        zero = jnp.zeros((BLOCKS, HALF), F32)
        er, ei = lax.fori_loop(0, STEPS, body, (zero, zero), unroll=4)
        for k in range(3):
            s = 1 << k
            qr = power_rows(pw_ref.at[2 * k], 8 * h, 8)
            qi = power_rows(pw_ref.at[2 * k + 1], 8 * h, 8)
            shr = jnp.where(sub >= s, pltpu.roll(er, s, 0), 0.0)
            shi = jnp.where(sub >= s, pltpu.roll(ei, s, 0), 0.0)
            dr, di = cmul(qr, qi, shr, shi)
            er, ei = er + dr, ei + di
        for k in range(8):
            fin_ref[pl.ds(8 * h + k, 1), :] = er[7:8, 128 * k : 128 * (k + 1)]
            fin_ref[pl.ds(16 + 8 * h + k, 1), :] = ei[7:8, 128 * k : 128 * (k + 1)]
        ent_ref[0, :, pl.ds(HALF * h, HALF)] = jnp.where(sub >= 1, pltpu.roll(er, 1, 0), 0.0)
        ent_ref[1, :, pl.ds(HALF * h, HALF)] = jnp.where(sub >= 1, pltpu.roll(ei, 1, 0), 0.0)

    fin = fin_ref[...].astype(BF16)
    for m in range(copies_ref.shape[0]):
        copies_ref[m] = fin


def horner(n, index, parts, wr, wi):
    tr, ti = jnp.zeros((LB, 128), F32), jnp.zeros((LB, 128), F32)
    br, bi = tr, ti
    pr, pi = tr + 1.0, ti
    ir, ii = pr, pi
    for k in range(n):
        here = index == k
        br, bi = jnp.where(here, tr, br), jnp.where(here, ti, bi)
        ir, ii = jnp.where(here, pr, ir), jnp.where(here, pi, ii)
        part = parts[k].astype(F32)
        mr, mi = cmul(wr, wi, tr, ti)
        tr, ti = mr + part[:LB], mi + part[LB:]
        pr, pi = cmul(wr, wi, pr, pi)
    return tr, ti, br, bi, ir, ii, pr, pi


def near_kernel(index_ref, parts_ref, whole_ref, copies_ref, near_ref):
    n = parts_ref.shape[0]
    tr, ti, br, bi, ir, ii, pr, pi = horner(
        n, index_ref[0], parts_ref, whole_ref[0], whole_ref[1]
    )
    for k, value in enumerate((br, bi, ir, ii, pr, pi)):
        near_ref[k] = value
    total = jnp.concatenate([tr, ti], axis=0).astype(BF16)
    for m in range(copies_ref.shape[0]):
        copies_ref[m] = total


def gelu(x):
    return 0.5 * x * (1.0 + jnp.tanh(0.7978845608028654 * (x + 0.044715 * (x * x * x))))


def second_kernel(
    index_ref, parts_ref, near_ref, ent_ref, up_ref, xr_ref, xi_ref, a_ref, f_ref,
    cr_ref, ci_ref, skip_ref, vw_hbm, gw_hbm,
    give_ref, keep_ref,
    sr_ref, si_ref, in_ref, dr_ref, di_ref, act_ref, vw_ref, gw_ref, sem,
):
    vcopy = pltpu.make_async_copy(vw_hbm, vw_ref, sem.at[0])
    gcopy = pltpu.make_async_copy(gw_hbm, gw_ref, sem.at[1])
    vcopy.start()
    gcopy.start()

    n = parts_ref.shape[0]
    _, _, gr, gi, _, _, _, _ = horner(n, index_ref[0], parts_ref, near_ref[4], near_ref[5])
    er, ei = cmul(near_ref[2], near_ref[3], gr, gi)
    in_ref[0], in_ref[1] = near_ref[0] + er, near_ref[1] + ei

    for g in range(G):
        rows = pl.ds(GROUP * g, GROUP)
        fr, fi = f_ref[0, pl.ds(g, 1), :], f_ref[1, pl.ds(g, 1), :]
        cr, ci = cr_ref[rows, :], ci_ref[rows, :]
        dr_ref[rows, :] = cr * fr - ci * fi
        di_ref[rows, :] = -(cr * fi + ci * fr)

    sub = lax.broadcasted_iota(jnp.int32, (BLOCKS, HALF), 0)
    for h in range(2):
        cols = pl.ds(HALF * h, HALF)
        mr, mi = power_rows(in_ref.at[0], 8 * h, 8), power_rows(in_ref.at[1], 8 * h, 8)
        for k in range(3):
            bit = (sub & (1 << k)) != 0
            qr = jnp.where(bit, power_rows(a_ref.at[2 + 2 * k], 8 * h, 8), 1.0)
            qi = jnp.where(bit, power_rows(a_ref.at[3 + 2 * k], 8 * h, 8), 0.0)
            mr, mi = cmul(qr, qi, mr, mi)
        er, ei = ent_ref[0, :, cols] + mr, ent_ref[1, :, cols] + mi
        mr, mi = power_rows(a_ref.at[0], 8 * h, 8), power_rows(a_ref.at[1], 8 * h, 8)

        def body(j, carried):
            hr, hi = carried
            rs, ims = [], []
            for step in range(2):
                rows = pl.ds(pl.multiple_of(j * 16, 16) + 8 * step, BLOCKS)
                nr, ni = cmul(mr, mi, hr, hi)
                hr = nr + xr_ref[rows, cols]
                hi = ni + xi_ref[rows, cols]
                rs.append(hr)
                ims.append(hi)
            rows = pl.ds(pl.multiple_of(j * 16, 16), 16)
            sr_ref[rows, cols] = jnp.concatenate(rs, axis=0).astype(BF16)
            si_ref[rows, cols] = jnp.concatenate(ims, axis=0).astype(BF16)
            return hr, hi

        lax.fori_loop(0, STEPS // 2, body, (er, ei), unroll=2)

    own = (lax.broadcasted_iota(jnp.int32, (128, 512), 0) >> 4) == (
        lax.broadcasted_iota(jnp.int32, (128, 512), 1) >> 6
    )
    for q in range(Q):
        total = skip_ref[:, pl.ds(128 * q, 128)] * up_ref[:, pl.ds(128 * q, 128)].astype(F32)
        for d_ref, s_ref in ((dr_ref, sr_ref), (di_ref, si_ref)):
            d = d_ref[pl.ds(128 * q, 128), :]
            wide = jnp.where(own, jnp.concatenate([d] * 8, axis=1), 0.0).astype(BF16)
            total = total + lax.dot_general(
                s_ref[:, pl.ds(512 * q, 512)], wide, (((1,), (1,)), ((), ())),
                preferred_element_type=F32,
            )
        act_ref[:, pl.ds(128 * q, 128)] = gelu(total).astype(BF16)

    act_ref[...] = jnp.dot(
        order_matrix(True), act_ref[...], preferred_element_type=F32
    ).astype(BF16)
    half = T // 2
    tp = index_ref[1]
    mine = act_ref[pl.ds(pl.multiple_of(tp * half, half), half), :]
    theirs = act_ref[pl.ds(pl.multiple_of((1 - tp) * half, half), half), :]
    width = vw_ref.shape[1]
    for copy, w_ref, k in ((vcopy, vw_ref, 0), (gcopy, gw_ref, 1)):
        copy.wait()
        for rows, out_ref in ((theirs, give_ref), (mine, keep_ref)):
            out_ref[:, pl.ds(width * k, width)] = jnp.dot(
                rows, w_ref[...], preferred_element_type=F32
            ).astype(BF16)


def call(kernel, outs, ins, scratch=(), name=None):
    return pl.pallas_call(
        kernel,
        out_shape=[jax.ShapeDtypeStruct(s, d) for s, d in outs],
        in_specs=[pl.BlockSpec(memory_space=m) for m in ins],
        out_specs=[pl.BlockSpec(memory_space=VMEM)] * len(outs),
        scratch_shapes=list(scratch),
        compiler_params=pltpu.CompilerParams(vmem_limit_bytes=56 * 1024 * 1024),
        name=name,
    )


def to_all(copies, axes):
    return lax.all_to_all(copies, axes, split_axis=0, concat_axis=0, tiled=True)


def local(
    features, lambda_real, lambda_imag, log_step, input_real, input_imag, real_output,
    imaginary_output, skip_gain, value_weight, gate_weight, value_bias, gate_bias,
):
    n_near = lax.axis_size("y") * lax.axis_size("x")
    n_far = lax.axis_size(FAR)
    near_index = lax.axis_index("y") * lax.axis_size("x") + lax.axis_index("x")
    far_index = lax.axis_index(FAR)
    tp = lax.axis_index("tp")
    near_at = jnp.stack([near_index]).astype(jnp.int32)
    far_at = jnp.stack([far_index, tp]).astype(jnp.int32)
    smem = pltpu.SMEM

    copies, whole, entering, up, xr, xi, powers, f = call(
        first_kernel,
        [
            ((n_near, 32, 128), BF16), ((2, LB, 128), F32), ((2, BLOCKS, FLAT), F32), ((T, CH), BF16),
            ((T, FLAT), F32), ((T, FLAT), F32), ((8, LB, 128), F32), ((2, G, STATE), F32),
        ],
        [VMEM, VMEM, VMEM, smem, VMEM, VMEM],
        [pltpu.VMEM((32, 128), F32), pltpu.VMEM((6, LB, 128), F32)],
        "first",
    )(
        features, lambda_real, lambda_imag, log_step,
        input_real.reshape(FLAT, GROUP), input_imag.reshape(FLAT, GROUP),
    )
    parts = to_all(copies, NEAR)
    totals, near = call(
        near_kernel,
        [((n_far, 32, 128), BF16), ((6, LB, 128), F32)],
        [smem, VMEM, VMEM],
        name="near",
    )(near_at, parts, whole)
    planes = to_all(totals, FAR)
    width = value_weight.shape[1]
    give, keep = call(
        second_kernel,
        [((T // 2, 2 * width), BF16), ((T // 2, 2 * width), BF16)],
        [smem] + [VMEM] * 11 + [pl.ANY] * 2,
        [
            pltpu.VMEM((T, FLAT), BF16), pltpu.VMEM((T, FLAT), BF16), pltpu.VMEM((2, LB, 128), F32),
            pltpu.VMEM((CH, STATE), F32), pltpu.VMEM((CH, STATE), F32), pltpu.VMEM((T, CH), BF16),
            pltpu.VMEM((CH, width), BF16), pltpu.VMEM((CH, width), BF16), pltpu.SemaphoreType.DMA((2,)),
        ],
        "second",
    )(
        far_at, planes, near, entering, up, xr, xi, powers, f,
        real_output.reshape(CH, STATE), imaginary_output.reshape(CH, STATE),
        skip_gain.reshape(1, CH), value_weight, gate_weight,
    )
    got = lax.ppermute(give, "tp", [(0, 1), (1, 0)])
    total = keep.astype(F32) + got.astype(F32)
    value_sum = total[:, :width] + value_bias
    gate_sum = total[:, width:] + gate_bias
    return (value_sum * jax.nn.sigmoid(gate_sum)).astype(BF16)


def solution(mesh):
    split = Mesh(mesh.devices.reshape(8, 8, 4, mesh.shape["tp"]), SP_TP)
    in_specs = (
        P(SP, "tp"),
        P("tp", None),
        P("tp", None),
        P("tp"),
        P("tp", None, None),
        P("tp", None, None),
        P("tp", None, None),
        P("tp", None, None),
        P("tp"),
        P("tp", None),
        P("tp", None),
        P(),
        P(),
    )
    return jax.shard_map(local, mesh=split, in_specs=in_specs, out_specs=P(SP_TP, None), check_vma=False)
```

time: 202 us -> 72 us (0.36)
  local copies, waits for them, and re-layouts: 70.1 us -> 5.91 us
  blocking collectives: 57.8 us -> 0 us
  other arithmetic: 27.7 us -> 3.18 us
  waiting for transfers between devices: 0.02 us -> 20.5 us
  Pallas kernels: 0 us -> 15.7 us
  between operations: 14.5 us -> 0.07 us
  matrix products: 9.82 us -> 0 us
  starting transfers between devices: 19.3 us -> 26.2 us
    all_gather x3 -> x0, blocking collectives: 57.8 us -> none  [gathered_once(): both, at, found = (lax.all_gather(jnp.concatenate(lines), axis), 0, {})]
    all_to_all x1 -> x2, waiting for transfers between devices: 0.01 us -> 18 us  [to_all(): return lax.all_to_all(copies, axes, split_axis=0, concat_axis=0, tiled=True)]
    pallas_call x0 -> x3, Pallas kernels: none -> 15.7 us  [the longest x1 6.97 us: local(): call(second_kernel, [((T // 2, 2 * width), BF16), ((T // 2, 2 * width), B...]
    dynamic_slice x32 -> x0, local copies, waits for them, and re-layouts: 14.6 us -> none  [block_carries(): lax.scan(advance, (start_re, start_im), (ends_re, ends_im))]
    slice x6 -> x0, local copies, waits for them, and re-layouts: 12 us -> none  [the longest x1 10.1 us: within_blocks(): new_re = step_re * h_re - step_im * h_im + blocks_re[:, offset]]
    unnamed x20 -> x0, other arithmetic: 11.6 us -> none
    transpose x2 -> x0, local copies, waits for them, and re-layouts: 10 us -> none  [the longest x1 5.55 us: local(): jnp.einsum('sgc,gpc->sgp', grouped, bar_re).reshape(positions, flat_width)]
    dot_general x6 -> x0, matrix products: 9.82 us -> none  [the longest x2 3.82 us: halves(): jnp.einsum('rnc,ncd->nrd', blocks_act, weight.reshape(pieces, slice_width...]
  transfers between devices with their start and end apart: 2 -> 3, of which waited for: 0 -> 3; matrix products, arithmetic and copies ran while one was open for 47% -> 1% of each run, Pallas kernels for 0% -> 0%
where the time goes in v1:
time: 72 us; the launch traced here: 71.6 us
  starting transfers between devices  26.2 us (36%)
  waiting for transfers between devices  20.5 us (28%)
  Pallas kernels  15.7 us (22%)
  local copies, waits for them, and re-layouts  5.91 us (8%)
  other arithmetic  3.18 us (4%)
    all_to_all x2, starting transfers between devices, to_all(): return lax.all_to_all(copies, axes, split_axis=0, concat_axis=0, tiled=True)  20.5 us
    all_to_all x2, waiting for transfers between devices, to_all(): return lax.all_to_all(copies, axes, split_axis=0, concat_axis=0, tiled=True)  18 us
    pallas_call x1, Pallas kernels, local(): call(second_kernel, [((T // 2, 2 * width), BF16), ((T // 2, 2 * width), B...  6.97 us
    pallas_call x1, Pallas kernels, local(): call(first_kernel, [((n_near, 32, 128), BF16), ((2, LB, 128), F32), ((2,...  6.91 us
    unnamed x10, local copies, waits for them, and re-layouts  5.91 us
    ppermute x1, starting transfers between devices, local(): got = lax.ppermute(give, 'tp', [(0, 1), (1, 0)])  5.69 us
    ppermute x1, waiting for transfers between devices, local(): got = lax.ppermute(give, 'tp', [(0, 1), (1, 0)])  2.48 us
    pallas_call x1, Pallas kernels, local(): call(near_kernel, [((n_far, 32, 128), BF16), ((6, LB, 128), F32)], [smem,...  1.78 us
  transfers between devices with their start and end apart: 3, of which 3 were waited for; matrix products, arithmetic and copies ran while one was open for 1% of the time, Pallas kernels for 0%

profile of v1, /device:TPU:1, one launch (start us, length us, event | category | flops | bytes accessed | tf_op | source)
XLA Modules:
  0.0 71.6 jit_solution(3011067681725192391)
XLA Ops:
  0.0 2.3 %copy.14 = f32[32,64,16]{2,1,0:T(8,128)} copy(f32[32,64,16]{1,2,0:T(8,128)} %param.17) | data formatting | bytes 262144 | tf_op args[4]
  2.3 2.3 %copy.15 = f32[32,64,16]{2,1,0:T(8,128)} copy(f32[32,64,16]{1,2,0:T(8,128)} %param.18) | data formatting | bytes 262144 | tf_op args[5]
  4.6 6.9 %first.1 = (bf16[32,32,128]{2,1,0:T(8,128)(2,1)}, f32[2,16,128]{2,1,0:T(8,128)}, f32[2,8,2048]{2,1,0:T(8,128)}, bf16[256,512]{1,0:T(8,128)(2,1)}, f32[256,2048]{...) custom-call(bf16[256,512]{1,0:T(8,128)(2,1)} %u_ref.1, f32[32,64]{1,0:T(8,128)} %lr_ref.1, ...), custom_call_target="tpu_custom_call" | custom-call | tf_op jit(solution)/shard_map/first/pallas_call | solution.py:291
  11.5 10.5 %all-to-all-start = ((bf16[32,32,128]{2,1,0:T(8,128)(2,1)}), bf16[32,32,128]{2,1,0:T(8,128)(2,1)S(1)}, u32[]{:S(2)}, u32[]{:S(2)}) async-start(bf16[32,32,128]{2,1,0:T(8,128)(2,1)} %get-tuple-element.17), calls=%async_computation | async-start | bytes 524288 | tf_op jit(solution)/shard_map/all_to_all | solution.py:275
  22.0 11.3 %all-to-all-done.parts_ref = bf16[32,32,128]{2,1,0:T(8,128)(2,1)S(1)} async-done(((bf16[32,32,128]{2,1,0:T(8,128)(2,1)}), bf16[32,32,128]{2,1,0:T(8,128)(2,1)S(1)}, u32[]{:S(2)}, u32[]{:S(2)}) %all-to-all-start) | async-done | bytes 262176 | tf_op jit(solution)/shard_map/all_to_all | solution.py:275
  33.3 0.0 copy-start
  33.3 0.7 copy-done
  34.0 1.8 %near.1 = (bf16[8,32,128]{2,1,0:T(8,128)(2,1)}, f32[6,16,128]{2,1,0:T(8,128)}) custom-call(s32[1]{0:T(128)} %bitcast.2.index_ref, bf16[32,32,128]{2,1,0:T(8,128)(2,1)} %copy-done, f32[2,16,128]{2,1,0:T(8,128)} %get-tuple-element.18.whole_ref), custom_call_target="tpu_custom_call" | custom-call | tf_op jit(solution)/shard_map/near/pallas_call | solution.py:305
  35.8 10.0 %all-to-all-start.1 = ((bf16[8,32,128]{2,1,0:T(8,128)(2,1)}), bf16[8,32,128]{2,1,0:T(8,128)(2,1)S(1)}, u32[]{:S(2)}, u32[]{:S(2)}) async-start(bf16[8,32,128]{2,1,0:T(8,128)(2,1)} %get-tuple-element.19), calls=%async_computation.1 | async-start | bytes 131072 | tf_op jit(solution)/shard_map/all_to_all | solution.py:275
  45.8 0.6 pad_add_fusion.index_ref
  46.4 6.7 %all-to-all-done.1.parts_ref = bf16[8,32,128]{2,1,0:T(8,128)(2,1)S(1)} async-done(((bf16[8,32,128]{2,1,0:T(8,128)(2,1)}), bf16[8,32,128]{2,1,0:T(8,128)(2,1)S(1)}, u32[]{:S(2)}, u32[]{:S(2)}) %all-to-all-start.1) | async-done | bytes 65568 | tf_op jit(solution)/shard_map/all_to_all | solution.py:275
  53.2 0.0 copy-start.1
  53.2 0.6 copy-done.1
  53.8 7.0 %second.1 = (bf16[128,4096]{1,0:T(8,128)(2,1)}, bf16[128,4096]{1,0:T(8,128)(2,1)}) custom-call(s32[2]{0:T(128)} %pad_add_fusion.index_ref, bf16[8,32,128]{2,1,0:T(8,128)(2,1)} %copy-done.1, f32[6,16,128]{2,1,0:T(8,128)} %get-tuple-element.20.near_ref, f32[2,8,2048]{2,1,0:T(8,128)} %get-tuple-element.21.ent_ref, bf16[256,512]{1,0:T(8,128)(2,1)} %get-tuple-element.22.up_ref, ...), custom_call_target="tpu_custom_call" | custom-call | tf_op jit(solution)/shard_map/second/pallas_call | solution.py:313
  60.8 5.7 %collective-permute-start = (bf16[128,4096]{1,0:T(8,128)(2,1)}, bf16[128,4096]{1,0:T(8,128)(2,1)S(1)}, u32[]{:S(2)}, u32[]{:S(2)}) collective-permute-start(bf16[128,4096]{1,0:T(8,128)(2,1)} %get-tuple-element.28), channel_id=1, source_target_pairs={{0,1},{1,0},{2,3},{3,2},{4,5},{5,4},{6,7},{7,6},{8,9},{9,8},{10,11... | collective-permute-start | bytes 3145736 | tf_op jit(solution)/shard_map/ppermute | solution.py:328
  66.5 2.5 %collective-permute-done = bf16[128,4096]{1,0:T(8,128)(2,1)S(1)} collective-permute-done((bf16[128,4096]{1,0:T(8,128)(2,1)}, bf16[128,4096]{1,0:T(8,128)(2,1)S(1)}, u32[]{:S(2)}, u32[]{:S(2)}) %collective-permute-start) | collective-permute-done | bytes 1048608 | tf_op jit(solution)/shard_map/ppermute | solution.py:328
  68.9 0.0 copy-start.2
  68.9 0.0 copy-start.3
  69.0 1.5 %convert_add_fusion = f32[128,4096]{1,0:T(8,128)S(1)} fusion(bf16[128,4096]{1,0:T(8,128)(2,1)S(1)} %collective-permute-done, bf16[128,4096]{1,0:T(8,128)(2,1)} %get-tuple-element.27), kind=kLoop, calls=%fused_computation | loop fusion | flops 1572864 | bytes 4194304 | tf_op jit(solution)/shard_map/add | solution.py:329
  70.5 0.0 copy-done.2
  70.5 0.0 copy-done.3
  70.5 1.1 %fusion.5 = bf16[128,2048]{1,0:T(8,128)(2,1)} fusion(f32[128,4096]{1,0:T(8,128)S(1)} %convert_add_fusion, f32[2048]{0:T(1024)S(1)} %copy-done.2, f32[2048]{0:T(1024)S(1)} %copy-done.3), kind=kLoop, calls=%fused_computation.8 | loop fusion | flops 1835008 | bytes 2637824 | tf_op jit(solution)/shard_map/convert_element_type | solution.py:332
Async XLA Ops:
  11.5 21.8 %all-to-all-start = ((bf16[32,32,128]{2,1,0:T(8,128)(2,1)}), bf16[32,32,128]{2,1,0:T(8,128)(2,1)S(1)}, u32[]{:S(2)}, u32[]{:S(2)}) async-start(bf16[32,32,128]{2,1,0:T(8,128)(2,1)} %get-tuple-element.17), calls=%async_computation | async-start | bytes 524288 | tf_op jit(solution)/shard_map/all_to_all | solution.py:275
  33.3 0.7 copy-start
  35.8 17.4 %all-to-all-start.1 = ((bf16[8,32,128]{2,1,0:T(8,128)(2,1)}), bf16[8,32,128]{2,1,0:T(8,128)(2,1)S(1)}, u32[]{:S(2)}, u32[]{:S(2)}) async-start(bf16[8,32,128]{2,1,0:T(8,128)(2,1)} %get-tuple-element.19), calls=%async_computation.1 | async-start | bytes 131072 | tf_op jit(solution)/shard_map/all_to_all | solution.py:275
  53.2 0.6 copy-start.1
  60.8 8.2 %collective-permute-start = (bf16[128,4096]{1,0:T(8,128)(2,1)}, bf16[128,4096]{1,0:T(8,128)(2,1)S(1)}, u32[]{:S(2)}, u32[]{:S(2)}) collective-permute-start(bf16[128,4096]{1,0:T(8,128)(2,1)} %get-tuple-element.28), channel_id=1, source_target_pairs={{0,1},{1,0},{2,3},{3,2},{4,5},{5,4},{6,7},{7,6},{8,9},{9,8},{10,11... | collective-permute-start | bytes 3145736 | tf_op jit(solution)/shard_map/ppermute | solution.py:328
  68.9 1.5 %copy-start.2 = (f32[2048]{0:T(1024)S(1)}, f32[2048]{0:T(1024)}, u32[]{:S(2)}) copy-start(f32[2048]{0:T(1024)} %param.25) | copy-start | bytes 24580
  68.9 1.5 %copy-start.3 = (f32[2048]{0:T(1024)S(1)}, f32[2048]{0:T(1024)}, u32[]{:S(2)}) copy-start(f32[2048]{0:T(1024)} %param.24) | copy-start | bytes 24580

commit v2 on v1

v2 whole, which is shorter than its diff:
```python
import jax
import jax.numpy as jnp
from jax import lax
from jax.experimental import pallas as pl
from jax.experimental.pallas import tpu as pltpu
from jax.sharding import Mesh
from jax.sharding import PartitionSpec as P

SP = ("z", "y", "x")
SP_TP = ("z", "y", "x", "tp")
NEAR = ("y", "x")
FAR = ("z", "tp")
SWAP = [(0, 1), (1, 0)]

T = 256
BLOCKS = 8
STEPS = 32
G = 32
STATE = 64
GROUP = 16
CH = 512
FLAT = 2048
LB = 16
HALF = 1024
Q = 4
HROWS = 128
HALF_D = CH // 2
PACK = 2 * CH + 4 * LB
CHUNK = 512

F32 = jnp.float32
BF16 = jnp.bfloat16
VMEM = pltpu.VMEM


def cmul(ar, ai, br, bi):
    return ar * br - ai * bi, ar * bi + ai * br


def power_rows(a_ref, lo, n):
    return jnp.concatenate(
        [jnp.broadcast_to(a_ref[pl.ds(lo + k, 1), :], (BLOCKS, 128)) for k in range(n)], axis=1
    )


def transition(lr_ref, li_ref, ls_ref):
    row = lax.broadcasted_iota(jnp.int32, (G, STATE), 0)
    logs = jnp.zeros((G, STATE), F32)
    for g in range(G):
        logs = jnp.where(row == g, ls_ref[g], logs)
    step = jnp.exp(logs)
    lr = lr_ref[...]
    li = li_ref[...]
    magnitude = jnp.exp(lr * step)
    phase = li * step
    return lr, li, magnitude * jnp.cos(phase), magnitude * jnp.sin(phase)


def order_matrix(transposed):
    r = lax.broadcasted_iota(jnp.int32, (T, T), 1 if transposed else 0)
    t = lax.broadcasted_iota(jnp.int32, (T, T), 0 if transposed else 1)
    hit = t == (r & 7) * STEPS + (r >> 3)
    return jnp.where(hit, 1.0, 0.0).astype(BF16)


def fold_groups(a):
    row = lax.broadcasted_iota(jnp.int32, (LB, G), 0)
    col = lax.broadcasted_iota(jnp.int32, (LB, G), 1)
    even = jnp.where(col == 2 * row, 1.0, 0.0)
    odd = jnp.where(col == 2 * row + 1, 1.0, 0.0)
    hi = lax.Precision.HIGHEST
    left = jnp.dot(even, a, precision=hi, preferred_element_type=F32)
    right = jnp.dot(odd, a, precision=hi, preferred_element_type=F32)
    return jnp.concatenate([left, right], axis=1)


def put_inputs(u, br_ref, bi_ref, xr_ref, xi_ref):
    up = jnp.dot(order_matrix(False), u, preferred_element_type=F32).astype(BF16)
    own = (lax.broadcasted_iota(jnp.int32, (128, 512), 0) >> 4) == (
        lax.broadcasted_iota(jnp.int32, (128, 512), 1) >> 6
    )
    for q in range(Q):
        for b_ref, x_ref in ((br_ref, xr_ref), (bi_ref, xi_ref)):
            b = b_ref[pl.ds(128 * q, 128), :]
            wide = jnp.where(own, jnp.concatenate([b] * 8, axis=1), 0.0).astype(BF16)
            x_ref[:, pl.ds(512 * q, 512)] = jnp.dot(
                up[:, 128 * q : 128 * (q + 1)], wide, preferred_element_type=F32
            )
    return up


def fetch(sources, targets, sem):
    moves = [
        pltpu.make_async_copy(src, dst, sem.at[k])
        for k, (src, dst) in enumerate(zip(sources, targets, strict=True))
    ]
    for move in moves:
        move.start()
    return moves


def first_kernel(
    ls_hbm, lr_hbm, li_hbm, u_hbm, br_hbm, bi_hbm,
    copies_ref, a_ref, ent_ref,
    xr_ref, xi_ref, fin_ref, pw_ref, ls_ref, lr_ref, li_ref, u_ref, br_ref, bi_ref, sem,
):
    moves = fetch(
        (ls_hbm, lr_hbm, li_hbm, u_hbm, br_hbm, bi_hbm),
        (ls_ref, lr_ref, li_ref, u_ref, br_ref, bi_ref), sem,
    )
    for move in moves[:3]:
        move.wait()
    _, _, ar, ai = transition(lr_ref, li_ref, ls_ref)
    pr, pi = fold_groups(ar), fold_groups(ai)
    a_ref[0], a_ref[1] = pr, pi
    for _ in range(5):
        pr, pi = cmul(pr, pi, pr, pi)
    for k in range(3):
        pw_ref[2 * k], pw_ref[2 * k + 1] = pr, pi
        pr, pi = cmul(pr, pi, pr, pi)
    a_ref[2], a_ref[3] = pr, pi
    for move in moves[3:]:
        move.wait()
    put_inputs(u_ref[...], br_ref, bi_ref, xr_ref, xi_ref)

    sub = lax.broadcasted_iota(jnp.int32, (BLOCKS, HALF), 0)
    for h in range(2):
        mr = power_rows(a_ref.at[0], 8 * h, 8)
        mi = power_rows(a_ref.at[1], 8 * h, 8)

        def body(j, carried):
            hr, hi = carried
            rows = pl.ds(pl.multiple_of(j * BLOCKS, BLOCKS), BLOCKS)
            nr, ni = cmul(mr, mi, hr, hi)
            nr = nr + xr_ref[rows, pl.ds(HALF * h, HALF)]
            ni = ni + xi_ref[rows, pl.ds(HALF * h, HALF)]
            return nr, ni

        zero = jnp.zeros((BLOCKS, HALF), F32)
        er, ei = lax.fori_loop(0, STEPS, body, (zero, zero), unroll=4)
        for k in range(3):
            s = 1 << k
            qr = power_rows(pw_ref.at[2 * k], 8 * h, 8)
            qi = power_rows(pw_ref.at[2 * k + 1], 8 * h, 8)
            shr = jnp.where(sub >= s, pltpu.roll(er, s, 0), 0.0)
            shi = jnp.where(sub >= s, pltpu.roll(ei, s, 0), 0.0)
            dr, di = cmul(qr, qi, shr, shi)
            er, ei = er + dr, ei + di
        for k in range(8):
            fin_ref[pl.ds(8 * h + k, 1), :] = er[7:8, 128 * k : 128 * (k + 1)]
            fin_ref[pl.ds(16 + 8 * h + k, 1), :] = ei[7:8, 128 * k : 128 * (k + 1)]
        ent_ref[0, :, pl.ds(HALF * h, HALF)] = jnp.where(sub >= 1, pltpu.roll(er, 1, 0), 0.0)
        ent_ref[1, :, pl.ds(HALF * h, HALF)] = jnp.where(sub >= 1, pltpu.roll(ei, 1, 0), 0.0)

    fin = fin_ref[...].astype(BF16)
    for m in range(copies_ref.shape[0]):
        copies_ref[m] = fin


def spread_pairs(parts):
    left = lax.broadcasted_iota(jnp.int32, (GROUP, 128), 1) < STATE
    zero = jnp.zeros((32, 128), BF16)
    rows = []
    for k, part in enumerate(parts):
        block = jnp.concatenate([jnp.where(left, part, 0.0), jnp.where(left, 0.0, part)], axis=0)
        rows.append(jnp.concatenate([block.astype(BF16) if j == k else zero for j in range(4)], axis=1))
    return jnp.concatenate(rows, axis=0)


def local_kernel(
    index_ref, ls_hbm, lr_hbm, li_hbm, cr_hbm, ci_hbm, u_hbm, br_hbm, bi_hbm, skip_hbm, a_ref, ent_ref,
    keep_ref, mine_ref, pack_ref,
    xr_ref, xi_ref, sr_ref, si_ref, y_ref,
    ls_ref, lr_ref, li_ref, cr_ref, ci_ref, u_ref, br_ref, bi_ref, skip_ref, sem,
):
    for move in fetch(
        (ls_hbm, lr_hbm, li_hbm, cr_hbm, ci_hbm, u_hbm, br_hbm, bi_hbm, skip_hbm),
        (ls_ref, lr_ref, li_ref, cr_ref, ci_ref, u_ref, br_ref, bi_ref, skip_ref), sem,
    ):
        move.wait()
    lr, li, ar, ai = transition(lr_ref, li_ref, ls_ref)
    den = lr * lr + li * li
    num = ar - 1.0
    fr = (num * lr + ai * li) / den
    fi = (ai * lr - num * li) / den
    for k in range(LB):
        pairs = []
        for g in (2 * k, 2 * k + 1):
            rows = pl.ds(GROUP * g, GROUP)
            pairs.append(cmul(cr_ref[rows, :], ci_ref[rows, :], fr[g : g + 1, :], fi[g : g + 1, :]))
        for c in range(2):
            d = jnp.concatenate([pairs[0][c], pairs[1][c]], axis=1)
            rows = pl.ds(HALF_D * c + GROUP * k, GROUP)
            mine_ref[rows, :] = d
            pack_ref[rows, :] = d
    for k in range(4):
        pack_ref[pl.ds(2 * CH + LB * k, LB), :] = a_ref[k]

    up = put_inputs(u_ref[...], br_ref, bi_ref, xr_ref, xi_ref)
    for h in range(2):
        cols = pl.ds(HALF * h, HALF)
        mr, mi = power_rows(a_ref.at[0], 8 * h, 8), power_rows(a_ref.at[1], 8 * h, 8)

        def body(j, carried):
            hr, hi = carried
            rs, ims = [], []
            for step in range(2):
                rows = pl.ds(pl.multiple_of(j * 16, 16) + 8 * step, BLOCKS)
                nr, ni = cmul(mr, mi, hr, hi)
                hr = nr + xr_ref[rows, cols]
                hi = ni + xi_ref[rows, cols]
                rs.append(hr)
                ims.append(hi)
            rows = pl.ds(pl.multiple_of(j * 16, 16), 16)
            sr_ref[rows, cols] = jnp.concatenate(rs, axis=0).astype(BF16)
            si_ref[rows, cols] = jnp.concatenate(ims, axis=0).astype(BF16)
            return hr, hi

        lax.fori_loop(0, STEPS // 2, body, (ent_ref[0, :, cols], ent_ref[1, :, cols]), unroll=2)

    for q in range(Q):
        cols = pl.ds(128 * q, 128)
        total = skip_ref[:, cols] * up[:, 128 * q : 128 * (q + 1)].astype(F32)
        for c, s_ref in enumerate((sr_ref, si_ref)):
            d = [mine_ref[pl.ds(HALF_D * c + GROUP * (4 * q + k), GROUP), :] for k in range(4)]
            wide = spread_pairs(d if c == 0 else [-part for part in d])
            total = total + lax.dot_general(
                s_ref[:, pl.ds(512 * q, 512)], wide, (((1,), (1,)), ((), ())),
                preferred_element_type=F32,
            )
        y_ref[:, cols] = total
    y_ref[...] = jnp.dot(
        order_matrix(True).astype(F32), y_ref[...],
        precision=lax.Precision.HIGHEST, preferred_element_type=F32,
    )
    tp = index_ref[2]
    mine = pl.ds(pl.multiple_of(tp * HROWS, HROWS), HROWS)
    theirs = pl.ds(pl.multiple_of((1 - tp) * HROWS, HROWS), HROWS)
    keep_ref[...] = y_ref[mine, :]
    for q in range(Q):
        pack_ref[pl.ds(CH + HROWS * q, HROWS), :] = y_ref[theirs, pl.ds(128 * q, 128)]


def near_kernel(index_ref, parts_ref, a_ref, copies_ref):
    wr, wi = a_ref[2], a_ref[3]
    index = index_ref[0]
    tr, ti = jnp.zeros((LB, 128), F32), jnp.zeros((LB, 128), F32)
    br, bi = tr, ti
    for k in range(parts_ref.shape[0]):
        here = index == k
        br, bi = jnp.where(here, tr, br), jnp.where(here, ti, bi)
        part = parts_ref[k].astype(F32)
        mr, mi = cmul(wr, wi, tr, ti)
        tr, ti = mr + part[:LB], mi + part[LB:]
    total = jnp.concatenate([tr, ti], axis=0).astype(BF16)
    before = jnp.concatenate([br, bi], axis=0).astype(BF16)
    for m in range(copies_ref.shape[0]):
        copies_ref[m] = jnp.where(index_ref[1] == m // 2, before, total)


def prepare_kernel(
    index_ref, mine_ref, other_ref,
    tr_ref, ti_ref, pw_ref,
    a_ref,
):
    near, tp = index_ref[0], index_ref[2]
    sub = lax.broadcasted_iota(jnp.int32, (BLOCKS, HALF), 0)
    for o in range(2):
        pack_ref, at = (mine_ref, 0) if o == 0 else (other_ref, 2 * CH)
        pr, pi, wr, wi = (
            pack_ref[k] if o == 0 else pack_ref[pl.ds(at + LB * k, LB), :] for k in range(4)
        )
        base = pr, pi
        pr, pi = wr, wi
        ir, ii = jnp.ones((LB, 128), F32), jnp.zeros((LB, 128), F32)
        for k in range(5):
            bit = ((near >> k) & 1) == 1
            jr, ji = cmul(ir, ii, pr, pi)
            ir, ii = jnp.where(bit, jr, ir), jnp.where(bit, ji, ii)
            pr, pi = cmul(pr, pi, pr, pi)
        pw_ref[o, 0], pw_ref[o, 1], pw_ref[o, 2], pw_ref[o, 3] = ir, ii, pr, pi

        pr, pi = base
        for k in range(8):
            a_ref[2 * k], a_ref[2 * k + 1] = pr, pi
            pr, pi = cmul(pr, pi, pr, pi)
        for h in range(2):
            cols = pl.ds(HALF * h, HALF)

            def power(k):
                return power_rows(a_ref.at[2 * k], 8 * h, 8), power_rows(a_ref.at[2 * k + 1], 8 * h, 8)

            mr, mi = power(0)
            for k, bit in ((0, (sub & 1) != 0), (1, (sub & 2) != 0), (2, (sub & 4) != 0), (7, tp == 1)):
                qr, qi = power(k)
                jr, ji = cmul(mr, mi, qr, qi)
                mr, mi = jnp.where(bit, jr, mr), jnp.where(bit, ji, mi)
            er, ei = power(3)

            def body(j, carried):
                hr, hi = carried
                nr, ni = cmul(er, ei, hr, hi)
                rows = pl.ds(pl.multiple_of(j * 16, 16), 16)
                tr_ref[o, rows, cols] = jnp.concatenate([hr, nr], axis=0).astype(BF16)
                ti_ref[o, rows, cols] = jnp.concatenate([hi, ni], axis=0).astype(BF16)
                return cmul(er, ei, nr, ni)

            lax.fori_loop(0, HROWS // 16, body, (mr, mi))


def gelu(x):
    return 0.5 * x * (1.0 + jnp.tanh(0.7978845608028654 * (x + 0.044715 * (x * x * x))))


def last_kernel(
    index_ref, parts_ref, keep_ref, mine_ref, other_ref, tr_ref, ti_ref, pw_ref,
    vw_hbm, gw_hbm, vo_hbm, go_hbm, vb_hbm, gb_hbm,
    out_ref,
    in_ref, act_ref, w_ref, vb_ref, gb_ref, sem,
):
    width = out_ref.shape[1]
    chunks = width // CHUNK
    moves = []
    for n in range(chunks):
        cols = pl.ds(CHUNK * n, CHUNK)
        for k, w_hbm in enumerate((vw_hbm, vo_hbm, gw_hbm, go_hbm)):
            moves.append(pltpu.make_async_copy(w_hbm.at[:, cols], w_ref.at[k, :, cols], sem.at[4 * n + k]))
    biases = [
        pltpu.make_async_copy(vb_hbm, vb_ref, sem.at[4 * chunks]),
        pltpu.make_async_copy(gb_hbm, gb_ref, sem.at[4 * chunks + 1]),
    ]
    for move in biases + moves:
        move.start()

    far, tp = index_ref[1], index_ref[2]
    n_far = parts_ref.shape[0] // 2
    for o in range(2):
        side = tp if o == 0 else 1 - tp
        wr, wi = pw_ref[o, 2], pw_ref[o, 3]
        gr, gi = jnp.zeros((LB, 128), F32), jnp.zeros((LB, 128), F32)
        for k in range(n_far - 1):
            part = parts_ref[2 * k + side].astype(F32)
            mr, mi = cmul(wr, wi, gr, gi)
            gr = jnp.where(k < far, mr + part[:LB], gr)
            gi = jnp.where(k < far, mi + part[LB:], gi)
        before = parts_ref[2 * far + side].astype(F32)
        mr, mi = cmul(pw_ref[o, 0], pw_ref[o, 1], gr, gi)
        in_ref[2 * o], in_ref[2 * o + 1] = before[:LB] + mr, before[LB:] + mi

    for o, d_ref in enumerate((mine_ref, other_ref)):
        for q in range(Q):
            real, imag = [], []
            for k in range(4 * q, 4 * q + 4):
                vr, vi = cmul(
                    d_ref[pl.ds(GROUP * k, GROUP), :], d_ref[pl.ds(HALF_D + GROUP * k, GROUP), :],
                    in_ref[2 * o, pl.ds(k, 1), :], in_ref[2 * o + 1, pl.ds(k, 1), :],
                )
                real.append(vr)
                imag.append(-vi)
            cols = pl.ds(128 * q, 128)
            total = keep_ref[:, cols] if o == 0 else other_ref[pl.ds(CH + HROWS * q, HROWS), :]
            for v, t_ref in ((real, tr_ref), (imag, ti_ref)):
                total = total + lax.dot_general(
                    t_ref[o, :, pl.ds(512 * q, 512)], spread_pairs(v), (((1,), (1,)), ((), ())),
                    preferred_element_type=F32,
                )
            act_ref[o, :, cols] = gelu(total).astype(BF16)

    def product(o, k, cols):
        return jnp.dot(act_ref[o], w_ref[k, :, cols], preferred_element_type=F32).astype(BF16).astype(F32)

    for move in biases:
        move.wait()
    for n in range(chunks):
        cols = pl.ds(CHUNK * n, CHUNK)
        for move in moves[4 * n : 4 * n + 4]:
            move.wait()
        value = product(0, 0, cols) + product(1, 1, cols) + vb_ref[:, cols]
        gate = product(0, 2, cols) + product(1, 3, cols) + gb_ref[:, cols]
        out_ref[:, cols] = (value * jax.nn.sigmoid(gate)).astype(BF16)


def call(kernel, outs, ins, scratch=(), limit=16):
    fn = pl.pallas_call(
        kernel,
        out_shape=[VMEM(s, d) if v else jax.ShapeDtypeStruct(s, d) for s, d, v in outs],
        in_specs=[pl.BlockSpec(memory_space=VMEM if m is True else m) for m in ins],
        out_specs=[pl.BlockSpec(memory_space=VMEM)] * len(outs),
        scratch_shapes=list(scratch),
        compiler_params=pltpu.CompilerParams(vmem_limit_bytes=limit * 1024 * 1024),
    )

    def run(*args):
        placed = []
        for a, m in zip(args, ins, strict=True):
            if m is True:
                a = pltpu.with_memory_space_constraint(a, VMEM)
            elif m is pltpu.HBM:
                a = pltpu.with_memory_space_constraint(a, pltpu.HBM)
            placed.append(a)
        return fn(*placed)

    return run


def to_all(copies, axes):
    return lax.all_to_all(copies, axes, split_axis=0, concat_axis=0, tiled=True)


def mixer(
    features, lambda_real, lambda_imag, log_step, input_real, input_imag, real_output,
    imaginary_output, skip_gain, value_weight, gate_weight, value_bias, gate_bias,
):
    n_near = lax.axis_size("y") * lax.axis_size("x")
    n_far = lax.axis_size("z")
    near_index = lax.axis_index("y") * lax.axis_size("x") + lax.axis_index("x")
    at = jnp.stack([near_index, lax.axis_index("z"), lax.axis_index("tp")]).astype(jnp.int32)
    smem, hbm = pltpu.SMEM, pltpu.HBM
    width = value_weight.shape[1]
    b_re = input_real.transpose(0, 2, 1).reshape(CH, STATE)
    b_im = input_imag.transpose(0, 2, 1).reshape(CH, STATE)
    params = (log_step, lambda_real, lambda_imag, b_re, b_im)
    rates = [smem((G,), F32), VMEM((G, STATE), F32), VMEM((G, STATE), F32)]
    matrix = [VMEM((CH, STATE), F32), VMEM((CH, STATE), F32)]

    copies, powers, entering = call(
        first_kernel,
        [((n_near, 32, 128), BF16, True), ((4, LB, 128), F32, True), ((2, BLOCKS, FLAT), F32, True)],
        [hbm] * 6,
        [
            VMEM((T, FLAT), F32), VMEM((T, FLAT), F32), VMEM((32, 128), F32), VMEM((6, LB, 128), F32),
            *rates, VMEM((T, CH), BF16), *matrix, pltpu.SemaphoreType.DMA((6,)),
        ],
        16,
    )(*params[:3], features, *params[3:])
    parts = to_all(copies, NEAR)
    keep, mine, pack = call(
        local_kernel,
        [((HROWS, CH), F32, True), ((CH, 128), F32, True), ((PACK, 128), F32, False)],
        [smem] + [hbm] * 9 + [True, True],
        [
            VMEM((T, FLAT), F32), VMEM((T, FLAT), F32), VMEM((T, FLAT), BF16), VMEM((T, FLAT), BF16),
            VMEM((T, CH), F32), *rates, *matrix, VMEM((T, CH), BF16), *matrix, VMEM((1, CH), F32),
            pltpu.SemaphoreType.DMA((9,)),
        ],
        20,
    )(
        at, *params[:3], real_output.reshape(CH, STATE), imaginary_output.reshape(CH, STATE),
        features, *params[3:], skip_gain.reshape(1, CH), powers, entering,
    )
    value_other = lax.ppermute(value_weight, "tp", SWAP)
    gate_other = lax.ppermute(gate_weight, "tp", SWAP)
    pack_other = lax.ppermute(pack, "tp", SWAP)
    (totals,) = call(near_kernel, [((2 * n_far, 32, 128), BF16, True)], [smem, True, True], limit=4)(at, parts, powers)
    planes = to_all(totals, FAR)
    prepared = call(
        prepare_kernel,
        [((2, HROWS, FLAT), BF16, True), ((2, HROWS, FLAT), BF16, True), ((2, 4, LB, 128), F32, True)],
        [smem, True, True],
        [VMEM((16, LB, 128), F32)],
    )(at, powers, pack_other)
    (out,) = call(
        last_kernel,
        [((HROWS, width), BF16, False)],
        [smem] + [True] * 7 + [hbm] * 6,
        [
            VMEM((4, LB, 128), F32), VMEM((2, HROWS, CH), BF16), VMEM((4, CH, width), BF16),
            VMEM((1, width), F32), VMEM((1, width), F32),
            pltpu.SemaphoreType.DMA((4 * (width // CHUNK) + 2,)),
        ],
        24,
    )(
        at, planes, keep, mine, pack_other, *prepared, value_weight, gate_weight, value_other, gate_other,
        value_bias.reshape(1, width), gate_bias.reshape(1, width),
    )
    return out


def solution(mesh):
    split = Mesh(mesh.devices.reshape(8, 8, 4, mesh.shape["tp"]), SP_TP)
    in_specs = (
        P(SP, "tp"),
        P("tp", None),
        P("tp", None),
        P("tp"),
        P("tp", None, None),
        P("tp", None, None),
        P("tp", None, None),
        P("tp", None, None),
        P("tp"),
        P("tp", None),
        P("tp", None),
        P(),
        P(),
    )
    return jax.shard_map(mixer, mesh=split, in_specs=in_specs, out_specs=P(SP_TP, None), check_vma=False)
```

time: 72 us -> 59.4 us (0.82)
  waiting for transfers between devices: 20.5 us -> 11.6 us
  local copies, waits for them, and re-layouts: 5.91 us -> 0 us
  starting transfers between devices: 26.2 us -> 30.2 us
  other arithmetic: 3.18 us -> 0.08 us
  Pallas kernels: 15.7 us -> 16.9 us
    ppermute x1 -> x3, starting transfers between devices: 5.69 us -> 13.3 us  [the longest x1 8.74 us: mixer(): value_other = lax.ppermute(value_weight, 'tp', SWAP)]
    all_to_all x2, waiting for transfers between devices: 18 us -> 11.6 us  [to_all(): return lax.all_to_all(copies, axes, split_axis=0, concat_axis=0, tiled=True)]
    unnamed x10 -> x0, local copies, waits for them, and re-layouts: 5.91 us -> none
    all_to_all x2, starting transfers between devices: 20.5 us -> 16.9 us  [to_all(): return lax.all_to_all(copies, axes, split_axis=0, concat_axis=0, tiled=True)]
    ppermute x1 -> x3, waiting for transfers between devices: 2.48 us -> 0.01 us  [the longest x1 0.01 us: mixer(): pack_other = lax.ppermute(pack, 'tp', SWAP)]
    add x1 -> x0, other arithmetic: 1.5 us -> none  [local(): total = keep.astype(F32) + got.astype(F32)]
    pallas_call x3 -> x5, Pallas kernels: 15.7 us -> 16.9 us  [run(): return fn(*placed)]
    convert_element_type x1 -> x0, other arithmetic: 1.08 us -> none  [local(): return (value_sum * jax.nn.sigmoid(gate_sum)).astype(BF16)]
  transfers between devices with their start and end apart: 3 -> 5, of which waited for: 3 -> 2; matrix products, arithmetic and copies ran while one was open for 1% -> 0% of each run, Pallas kernels for 0% -> 18%
where the time goes in v2:
time: 59.4 us; the launch traced here: 59 us
  starting transfers between devices  30.2 us (51%)
  Pallas kernels  16.9 us (28%)
  waiting for transfers between devices  11.6 us (20%)
    pallas_call x5, Pallas kernels, run(): return fn(*placed)  16.9 us
    all_to_all x2, starting transfers between devices, to_all(): return lax.all_to_all(copies, axes, split_axis=0, concat_axis=0, tiled=True)  16.9 us
    all_to_all x2, waiting for transfers between devices, to_all(): return lax.all_to_all(copies, axes, split_axis=0, concat_axis=0, tiled=True)  11.6 us
    ppermute x1, starting transfers between devices, mixer(): value_other = lax.ppermute(value_weight, 'tp', SWAP)  8.74 us
    ppermute x1, starting transfers between devices, mixer(): pack_other = lax.ppermute(pack, 'tp', SWAP)  2.68 us
    ppermute x1, starting transfers between devices, mixer(): gate_other = lax.ppermute(gate_weight, 'tp', SWAP)  1.92 us
  transfers between devices with their start and end apart: 5, of which 2 were waited for; matrix products, arithmetic and copies ran while one was open for 0% of the time, Pallas kernels for 18%

profile of v2, /device:TPU:1, one launch (start us, length us, event | category | flops | bytes accessed | tf_op | source)
XLA Modules:
  0.0 59.0 jit_solution(2432786276184335260)
XLA Ops:
  0.0 8.7 %collective-permute-start.1 = (bf16[512,2048]{1,0:T(8,128)(2,1)}, bf16[512,2048]{1,0:T(8,128)(2,1)}, u32[]{:S(2)}, u32[]{:S(2)}) collective-permute-start(bf16[512,2048]{1,0:T(8,128)(2,1)} %vw_hbm.1), channel_id=1, source_target_pairs={{0,1},{1,0},{2,3},{3,2},{4,5},{5,4},{6,7},{7,6},{8,9},{9,8},{10,11... | collective-permute-start | bytes 6291464 | tf_op jit(solution)/shard_map/ppermute | solution.py:451
  8.7 1.9 %collective-permute-start.2 = (bf16[512,2048]{1,0:T(8,128)(2,1)}, bf16[512,2048]{1,0:T(8,128)(2,1)}, u32[]{:S(2)}, u32[]{:S(2)}) collective-permute-start(bf16[512,2048]{1,0:T(8,128)(2,1)} %gw_hbm.1), channel_id=1, source_target_pairs={{0,1},{1,0},{2,3},{3,2},{4,5},{5,4},{6,7},{7,6},{8,9},{9,8},{10,11... | collective-permute-start | bytes 6291464 | tf_op jit(solution)/shard_map/ppermute | solution.py:452
  10.7 3.5 %shard_map.127 = (bf16[32,32,128]{2,1,0:T(8,128)(2,1)}, f32[4,16,128]{2,1,0:T(8,128)S(1)}, f32[2,8,2048]{2,1,0:T(8,128)S(1)}) custom-call(f32[32]{0:T(128)} %ls_hbm.3, f32[32,64]{1,0:T(8,128)} %lr_hbm.3, f32[32,64]{1,0:T(8,128)} %li_hbm.3, bf16[256,512]{1,0:T(8,128)(2,1)} %u_hbm.3, f32[512,64]{1,0:T(8,128)} %bitcast.14, f32[512,64]{1,0:T(8,128)} %bitcast.16), custom_call_target="tpu_custom_call" | custom-call | tf_op jit(solution)/shard_map/pallas_call | solution.py:401
  14.2 4.3 %all-to-all-start = ((bf16[32,32,128]{2,1,0:T(8,128)(2,1)}), bf16[32,32,128]{2,1,0:T(8,128)(2,1)S(1)}, u32[]{:S(2)}, u32[]{:S(2)}) async-start(bf16[32,32,128]{2,1,0:T(8,128)(2,1)} %get-tuple-element.14), calls=%async_computation | async-start | bytes 524288 | tf_op jit(solution)/shard_map/all_to_all | solution.py:407
  18.5 0.1 pad_add_fusion.index_ref
  18.6 4.8 %shard_map.129 = (f32[128,512]{1,0:T(8,128)S(1)}, f32[512,128]{1,0:T(8,128)S(1)}, f32[1088,128]{1,0:T(8,128)S(1)}) custom-call(s32[3]{0:T(128)S(1)} %pad_add_fusion.index_ref, f32[32]{0:T(128)} %ls_hbm.3, f32[32,64]{1,0:T(8,128)} %lr_hbm.3, f32[32,64]{1,0:T(8,128)} %li_hbm.3, f32[512,64]{1,0:T(8,128)} %bitcast.18, f32[512,64]{1,0:T(8,128)} %bitcast.19, ...), custom_call_target="tpu_custom_call" | custom-call | tf_op jit(solution)/shard_map/pallas_call | solution.py:401
  23.3 2.7 %collective-permute-start = (f32[1088,128]{1,0:T(8,128)S(1)}, f32[1088,128]{1,0:T(8,128)S(1)}, u32[]{:S(2)}, u32[]{:S(2)}) collective-permute-start(f32[1088,128]{1,0:T(8,128)S(1)} %get-tuple-element.19), channel_id=1, source_target_pairs={{0,1},{1,0},{2,3},{3,2},{4,5},{5,4},{6,7},{7,6},{8,9},{9,8},{10,11... | collective-permute-start | bytes 1671176 | tf_op jit(solution)/shard_map/ppermute | solution.py:453
  26.0 4.0 %all-to-all-done.parts_ref = bf16[32,32,128]{2,1,0:T(8,128)(2,1)S(1)} async-done(((bf16[32,32,128]{2,1,0:T(8,128)(2,1)}), bf16[32,32,128]{2,1,0:T(8,128)(2,1)S(1)}, u32[]{:S(2)}, u32[]{:S(2)}) %all-to-all-start) | async-done | bytes 262176 | tf_op jit(solution)/shard_map/all_to_all | solution.py:407
  30.1 1.3 %shard_map.128 = bf16[16,32,128]{2,1,0:T(8,128)(2,1)} custom-call(s32[3]{0:T(128)S(1)} %pad_add_fusion.index_ref, bf16[32,32,128]{2,1,0:T(8,128)(2,1)S(1)} %all-to-all-done.parts_ref, f32[4,16,128]{2,1,0:T(8,128)S(1)} %get-tuple-element.15.a_ref.mine_ref), custom_call_target="tpu_custom_call" | custom-call | tf_op jit(solution)/shard_map/pallas_call | solution.py:401
  31.4 12.6 %all-to-all-start.1 = ((bf16[16,32,128]{2,1,0:T(8,128)(2,1)}), bf16[16,32,128]{2,1,0:T(8,128)(2,1)S(1)}, u32[]{:S(2)}, u32[]{:S(2)}) async-start(bf16[16,32,128]{2,1,0:T(8,128)(2,1)} %shard_map.128), calls=%async_computation.1 | async-start | bytes 262144 | tf_op jit(solution)/shard_map/all_to_all | solution.py:407
  44.0 0.0 collective-permute-done.other_ref
  44.0 1.3 %shard_map.130 = (bf16[2,128,2048]{2,1,0:T(8,128)(2,1)S(1)}, bf16[2,128,2048]{2,1,0:T(8,128)(2,1)S(1)}, f32[2,4,16,128]{3,2,1,0:T(8,128)S(1)}) custom-call(s32[3]{0:T(128)S(1)} %pad_add_fusion.index_ref, f32[4,16,128]{2,1,0:T(8,128)S(1)} %get-tuple-element.15.a_ref.mine_ref, f32[1088,128]{1,0:T(8,128)S(1)} %collective-permute-done.other_ref), custom_call_target="tpu_custom_call" | custom-call | tf_op jit(solution)/shard_map/pallas_call | solution.py:401
  45.3 7.6 %all-to-all-done.1.parts_ref = bf16[16,32,128]{2,1,0:T(8,128)(2,1)S(1)} async-done(((bf16[16,32,128]{2,1,0:T(8,128)(2,1)}), bf16[16,32,128]{2,1,0:T(8,128)(2,1)S(1)}, u32[]{:S(2)}, u32[]{:S(2)}) %all-to-all-start.1) | async-done | bytes 131104 | tf_op jit(solution)/shard_map/all_to_all | solution.py:407
  52.9 0.0 collective-permute-done.1.vo_hbm
  52.9 0.0 collective-permute-done.2.go_hbm
  52.9 6.1 %shard_map.131 = bf16[128,2048]{1,0:T(8,128)(2,1)} custom-call(s32[3]{0:T(128)S(1)} %pad_add_fusion.index_ref, bf16[16,32,128]{2,1,0:T(8,128)(2,1)S(1)} %all-to-all-done.1.parts_ref, f32[128,512]{1,0:T(8,128)S(1)} %get-tuple-element.17.keep_ref, f32[512,128]{1,0:T(8,128)S(1)} %get-tuple-element.18.mine_ref, f32[1088,128]{1,0:T(8,128)S(1)} %collective-permute-done.other_ref, ...), custom_call_target="tpu_custom_call" | custom-call | tf_op jit(solution)/shard_map/pallas_call | solution.py:401
Async XLA Ops:
  0.0 52.9 %collective-permute-start.1 = (bf16[512,2048]{1,0:T(8,128)(2,1)}, bf16[512,2048]{1,0:T(8,128)(2,1)}, u32[]{:S(2)}, u32[]{:S(2)}) collective-permute-start(bf16[512,2048]{1,0:T(8,128)(2,1)} %vw_hbm.1), channel_id=1, source_target_pairs={{0,1},{1,0},{2,3},{3,2},{4,5},{5,4},{6,7},{7,6},{8,9},{9,8},{10,11... | collective-permute-start | bytes 6291464 | tf_op jit(solution)/shard_map/ppermute | solution.py:451
  8.7 44.1 %collective-permute-start.2 = (bf16[512,2048]{1,0:T(8,128)(2,1)}, bf16[512,2048]{1,0:T(8,128)(2,1)}, u32[]{:S(2)}, u32[]{:S(2)}) collective-permute-start(bf16[512,2048]{1,0:T(8,128)(2,1)} %gw_hbm.1), channel_id=1, source_target_pairs={{0,1},{1,0},{2,3},{3,2},{4,5},{5,4},{6,7},{7,6},{8,9},{9,8},{10,11... | collective-permute-start | bytes 6291464 | tf_op jit(solution)/shard_map/ppermute | solution.py:452
  14.2 15.9 %all-to-all-start = ((bf16[32,32,128]{2,1,0:T(8,128)(2,1)}), bf16[32,32,128]{2,1,0:T(8,128)(2,1)S(1)}, u32[]{:S(2)}, u32[]{:S(2)}) async-start(bf16[32,32,128]{2,1,0:T(8,128)(2,1)} %get-tuple-element.14), calls=%async_computation | async-start | bytes 524288 | tf_op jit(solution)/shard_map/all_to_all | solution.py:407
  23.3 20.6 %collective-permute-start = (f32[1088,128]{1,0:T(8,128)S(1)}, f32[1088,128]{1,0:T(8,128)S(1)}, u32[]{:S(2)}, u32[]{:S(2)}) collective-permute-start(f32[1088,128]{1,0:T(8,128)S(1)} %get-tuple-element.19), channel_id=1, source_target_pairs={{0,1},{1,0},{2,3},{3,2},{4,5},{5,4},{6,7},{7,6},{8,9},{9,8},{10,11... | collective-permute-start | bytes 1671176 | tf_op jit(solution)/shard_map/ppermute | solution.py:453
  31.4 21.5 %all-to-all-start.1 = ((bf16[16,32,128]{2,1,0:T(8,128)(2,1)}), bf16[16,32,128]{2,1,0:T(8,128)(2,1)S(1)}, u32[]{:S(2)}, u32[]{:S(2)}) async-start(bf16[16,32,128]{2,1,0:T(8,128)(2,1)} %shard_map.128), calls=%async_computation.1 | async-start | bytes 262144 | tf_op jit(solution)/shard_map/all_to_all | solution.py:407

commit v3 on v2

--- a/solution.py
+++ b/solution.py
@@ -74,6 +74,10 @@
     return jnp.concatenate([left, right], axis=1)
 
 
+def near_index():
+    return lax.axis_index("y") * lax.axis_size("x") + lax.axis_index("x")
+
+
 def put_inputs(u, br_ref, bi_ref, xr_ref, xi_ref):
     up = jnp.dot(order_matrix(False), u, preferred_element_type=F32).astype(BF16)
     own = (lax.broadcasted_iota(jnp.int32, (128, 512), 0) >> 4) == (
@@ -168,7 +172,7 @@
 
 
 def local_kernel(
-    index_ref, ls_hbm, lr_hbm, li_hbm, cr_hbm, ci_hbm, u_hbm, br_hbm, bi_hbm, skip_hbm, a_ref, ent_ref,
+    ls_hbm, lr_hbm, li_hbm, cr_hbm, ci_hbm, u_hbm, br_hbm, bi_hbm, skip_hbm, a_ref, ent_ref,
     keep_ref, mine_ref, pack_ref,
     xr_ref, xi_ref, sr_ref, si_ref, y_ref,
     ls_ref, lr_ref, li_ref, cr_ref, ci_ref, u_ref, br_ref, bi_ref, skip_ref, sem,
@@ -229,11 +233,14 @@
                 preferred_element_type=F32,
             )
         y_ref[:, cols] = total
-    y_ref[...] = jnp.dot(
-        order_matrix(True).astype(F32), y_ref[...],
-        precision=lax.Precision.HIGHEST, preferred_element_type=F32,
-    )
-    tp = index_ref[2]
+    back = order_matrix(True)
+    y = y_ref[...]
+    high = y.astype(BF16)
+    low = (y - high.astype(F32)).astype(BF16)
+    y_ref[...] = jnp.dot(back, high, preferred_element_type=F32) + jnp.dot(
+        back, low, preferred_element_type=F32
+    )
+    tp = lax.axis_index("tp")
     mine = pl.ds(pl.multiple_of(tp * HROWS, HROWS), HROWS)
     theirs = pl.ds(pl.multiple_of((1 - tp) * HROWS, HROWS), HROWS)
     keep_ref[...] = y_ref[mine, :]
@@ -241,9 +248,10 @@
         pack_ref[pl.ds(CH + HROWS * q, HROWS), :] = y_ref[theirs, pl.ds(128 * q, 128)]
 
 
-def near_kernel(index_ref, parts_ref, a_ref, copies_ref):
+def near_kernel(parts_ref, a_ref, copies_ref):
     wr, wi = a_ref[2], a_ref[3]
-    index = index_ref[0]
+    index = near_index()
+    plane = lax.axis_index("z")
     tr, ti = jnp.zeros((LB, 128), F32), jnp.zeros((LB, 128), F32)
     br, bi = tr, ti
     for k in range(parts_ref.shape[0]):
@@ -255,57 +263,52 @@
     total = jnp.concatenate([tr, ti], axis=0).astype(BF16)
     before = jnp.concatenate([br, bi], axis=0).astype(BF16)
     for m in range(copies_ref.shape[0]):
-        copies_ref[m] = jnp.where(index_ref[1] == m // 2, before, total)
-
-
-def prepare_kernel(
-    index_ref, mine_ref, other_ref,
-    tr_ref, ti_ref, pw_ref,
-    a_ref,
-):
-    near, tp = index_ref[0], index_ref[2]
+        copies_ref[m] = jnp.where(plane == m // 2, before, total)
+
+
+def load_kernel(w_hbm, w_ref, sem):
+    move = pltpu.make_async_copy(w_hbm, w_ref, sem.at[0])
+    move.start()
+    move.wait()
+
+
+def power_tables(o, base, whole, tr_ref, ti_ref, pw_ref, a_ref):
+    near, tp = near_index(), lax.axis_index("tp")
     sub = lax.broadcasted_iota(jnp.int32, (BLOCKS, HALF), 0)
-    for o in range(2):
-        pack_ref, at = (mine_ref, 0) if o == 0 else (other_ref, 2 * CH)
-        pr, pi, wr, wi = (
-            pack_ref[k] if o == 0 else pack_ref[pl.ds(at + LB * k, LB), :] for k in range(4)
-        )
-        base = pr, pi
-        pr, pi = wr, wi
-        ir, ii = jnp.ones((LB, 128), F32), jnp.zeros((LB, 128), F32)
-        for k in range(5):
-            bit = ((near >> k) & 1) == 1
-            jr, ji = cmul(ir, ii, pr, pi)
-            ir, ii = jnp.where(bit, jr, ir), jnp.where(bit, ji, ii)
-            pr, pi = cmul(pr, pi, pr, pi)
-        pw_ref[o, 0], pw_ref[o, 1], pw_ref[o, 2], pw_ref[o, 3] = ir, ii, pr, pi
-
-        pr, pi = base
-        for k in range(8):
-            a_ref[2 * k], a_ref[2 * k + 1] = pr, pi
-            pr, pi = cmul(pr, pi, pr, pi)
-        for h in range(2):
-            cols = pl.ds(HALF * h, HALF)
-
-            def power(k):
-                return power_rows(a_ref.at[2 * k], 8 * h, 8), power_rows(a_ref.at[2 * k + 1], 8 * h, 8)
-
-            mr, mi = power(0)
-            for k, bit in ((0, (sub & 1) != 0), (1, (sub & 2) != 0), (2, (sub & 4) != 0), (7, tp == 1)):
-                qr, qi = power(k)
-                jr, ji = cmul(mr, mi, qr, qi)
-                mr, mi = jnp.where(bit, jr, mr), jnp.where(bit, ji, mi)
-            er, ei = power(3)
-
-            def body(j, carried):
-                hr, hi = carried
-                nr, ni = cmul(er, ei, hr, hi)
-                rows = pl.ds(pl.multiple_of(j * 16, 16), 16)
-                tr_ref[o, rows, cols] = jnp.concatenate([hr, nr], axis=0).astype(BF16)
-                ti_ref[o, rows, cols] = jnp.concatenate([hi, ni], axis=0).astype(BF16)
-                return cmul(er, ei, nr, ni)
-
-            lax.fori_loop(0, HROWS // 16, body, (mr, mi))
+    pr, pi = whole
+    ir, ii = jnp.ones((LB, 128), F32), jnp.zeros((LB, 128), F32)
+    for k in range(5):
+        bit = ((near >> k) & 1) == 1
+        jr, ji = cmul(ir, ii, pr, pi)
+        ir, ii = jnp.where(bit, jr, ir), jnp.where(bit, ji, ii)
+        pr, pi = cmul(pr, pi, pr, pi)
+    pw_ref[o, 0], pw_ref[o, 1], pw_ref[o, 2], pw_ref[o, 3] = ir, ii, pr, pi
+    pr, pi = base
+    for k in range(8):
+        a_ref[2 * k], a_ref[2 * k + 1] = pr, pi
+        pr, pi = cmul(pr, pi, pr, pi)
+    for h in range(2):
+        cols = pl.ds(HALF * h, HALF)
+
+        def power(k):
+            return power_rows(a_ref.at[2 * k], 8 * h, 8), power_rows(a_ref.at[2 * k + 1], 8 * h, 8)
+
+        mr, mi = power(0)
+        for k, bit in ((0, (sub & 1) != 0), (1, (sub & 2) != 0), (2, (sub & 4) != 0), (7, tp == 1)):
+            qr, qi = power(k)
+            jr, ji = cmul(mr, mi, qr, qi)
+            mr, mi = jnp.where(bit, jr, mr), jnp.where(bit, ji, mi)
+        er, ei = power(3)
+
+        def body(j, carried):
+            hr, hi = carried
+            nr, ni = cmul(er, ei, hr, hi)
+            rows = pl.ds(pl.multiple_of(j * 16, 16), 16)
+            tr_ref[o, rows, cols] = jnp.concatenate([hr, nr], axis=0).astype(BF16)
+            ti_ref[o, rows, cols] = jnp.concatenate([hi, ni], axis=0).astype(BF16)
+            return cmul(er, ei, nr, ni)
+
+        lax.fori_loop(0, HROWS // 16, body, (mr, mi))
 
 
 def gelu(x):
@@ -313,26 +316,30 @@
 
 
 def last_kernel(
-    index_ref, parts_ref, keep_ref, mine_ref, other_ref, tr_ref, ti_ref, pw_ref,
-    vw_hbm, gw_hbm, vo_hbm, go_hbm, vb_hbm, gb_hbm,
-    out_ref,
-    in_ref, act_ref, w_ref, vb_ref, gb_ref, sem,
+    parts_ref, keep_ref, mine_ref, other_ref, powers_ref, vw_ref,
+    gw_hbm, vo_hbm, go_hbm, vb_hbm, gb_hbm,
+    out_hbm,
+    in_ref, act_ref, out_ref, w_ref, vb_ref, gb_ref, tr_ref, ti_ref, pw_ref, a_ref, sem,
 ):
     width = out_ref.shape[1]
     chunks = width // CHUNK
-    moves = []
+    moves, results = [], []
     for n in range(chunks):
         cols = pl.ds(CHUNK * n, CHUNK)
-        for k, w_hbm in enumerate((vw_hbm, vo_hbm, gw_hbm, go_hbm)):
-            moves.append(pltpu.make_async_copy(w_hbm.at[:, cols], w_ref.at[k, :, cols], sem.at[4 * n + k]))
+        for k, w_hbm in enumerate((vo_hbm, gw_hbm, go_hbm)):
+            moves.append(pltpu.make_async_copy(w_hbm.at[:, cols], w_ref.at[k, :, cols], sem.at[3 * n + k]))
     biases = [
-        pltpu.make_async_copy(vb_hbm, vb_ref, sem.at[4 * chunks]),
-        pltpu.make_async_copy(gb_hbm, gb_ref, sem.at[4 * chunks + 1]),
+        pltpu.make_async_copy(vb_hbm, vb_ref, sem.at[3 * chunks]),
+        pltpu.make_async_copy(gb_hbm, gb_ref, sem.at[3 * chunks + 1]),
     ]
     for move in biases + moves:
         move.start()
 
-    far, tp = index_ref[1], index_ref[2]
+    for o in range(2):
+        both = [powers_ref[k] if o == 0 else other_ref[pl.ds(2 * CH + LB * k, LB), :] for k in range(4)]
+        power_tables(o, both[:2], both[2:], tr_ref, ti_ref, pw_ref, a_ref)
+
+    far, tp = lax.axis_index("z"), lax.axis_index("tp")
     n_far = parts_ref.shape[0] // 2
     for o in range(2):
         side = tp if o == 0 else 1 - tp
@@ -367,17 +374,24 @@
             act_ref[o, :, cols] = gelu(total).astype(BF16)
 
     def product(o, k, cols):
-        return jnp.dot(act_ref[o], w_ref[k, :, cols], preferred_element_type=F32).astype(BF16).astype(F32)
+        w = vw_ref[:, cols] if k < 0 else w_ref[k, :, cols]
+        return jnp.dot(act_ref[o], w, preferred_element_type=F32).astype(BF16).astype(F32)
 
     for move in biases:
         move.wait()
     for n in range(chunks):
         cols = pl.ds(CHUNK * n, CHUNK)
-        for move in moves[4 * n : 4 * n + 4]:
+        for move in moves[3 * n : 3 * n + 3]:
             move.wait()
-        value = product(0, 0, cols) + product(1, 1, cols) + vb_ref[:, cols]
-        gate = product(0, 2, cols) + product(1, 3, cols) + gb_ref[:, cols]
+        value = product(0, -1, cols) + product(1, 0, cols) + vb_ref[:, cols]
+        gate = product(0, 1, cols) + product(1, 2, cols) + gb_ref[:, cols]
         out_ref[:, cols] = (value * jax.nn.sigmoid(gate)).astype(BF16)
+        results.append(
+            pltpu.make_async_copy(out_ref.at[:, cols], out_hbm.at[:, cols], sem.at[3 * chunks + 2 + n])
+        )
+        results[-1].start()
+    for move in results:
+        move.wait()
 
 
 def call(kernel, outs, ins, scratch=(), limit=16):
@@ -385,7 +399,7 @@
         kernel,
         out_shape=[VMEM(s, d) if v else jax.ShapeDtypeStruct(s, d) for s, d, v in outs],
         in_specs=[pl.BlockSpec(memory_space=VMEM if m is True else m) for m in ins],
-        out_specs=[pl.BlockSpec(memory_space=VMEM)] * len(outs),
+        out_specs=[pl.BlockSpec(memory_space=pltpu.HBM if v is None else VMEM) for _, _, v in outs],
         scratch_shapes=list(scratch),
         compiler_params=pltpu.CompilerParams(vmem_limit_bytes=limit * 1024 * 1024),
     )
@@ -413,8 +427,6 @@
 ):
     n_near = lax.axis_size("y") * lax.axis_size("x")
     n_far = lax.axis_size("z")
-    near_index = lax.axis_index("y") * lax.axis_size("x") + lax.axis_index("x")
-    at = jnp.stack([near_index, lax.axis_index("z"), lax.axis_index("tp")]).astype(jnp.int32)
     smem, hbm = pltpu.SMEM, pltpu.HBM
     width = value_weight.shape[1]
     b_re = input_real.transpose(0, 2, 1).reshape(CH, STATE)
@@ -434,43 +446,43 @@
         16,
     )(*params[:3], features, *params[3:])
     parts = to_all(copies, NEAR)
-    keep, mine, pack = call(
+    local_call = call(
         local_kernel,
         [((HROWS, CH), F32, True), ((CH, 128), F32, True), ((PACK, 128), F32, False)],
-        [smem] + [hbm] * 9 + [True, True],
+        [hbm] * 9 + [True, True],
         [
             VMEM((T, FLAT), F32), VMEM((T, FLAT), F32), VMEM((T, FLAT), BF16), VMEM((T, FLAT), BF16),
             VMEM((T, CH), F32), *rates, *matrix, VMEM((T, CH), BF16), *matrix, VMEM((1, CH), F32),
             pltpu.SemaphoreType.DMA((9,)),
         ],
         20,
-    )(
-        at, *params[:3], real_output.reshape(CH, STATE), imaginary_output.reshape(CH, STATE),
+    )
+    keep, mine, pack = local_call(
+        *params[:3], real_output.reshape(CH, STATE), imaginary_output.reshape(CH, STATE),
         features, *params[3:], skip_gain.reshape(1, CH), powers, entering,
     )
     value_other = lax.ppermute(value_weight, "tp", SWAP)
     gate_other = lax.ppermute(gate_weight, "tp", SWAP)
     pack_other = lax.ppermute(pack, "tp", SWAP)
-    (totals,) = call(near_kernel, [((2 * n_far, 32, 128), BF16, True)], [smem, True, True], limit=4)(at, parts, powers)
+    near_call = call(near_kernel, [((2 * n_far, 32, 128), BF16, True)], [True, True], limit=4)
+    (totals,) = near_call(parts, powers)
     planes = to_all(totals, FAR)
-    prepared = call(
-        prepare_kernel,
-        [((2, HROWS, FLAT), BF16, True), ((2, HROWS, FLAT), BF16, True), ((2, 4, LB, 128), F32, True)],
-        [smem, True, True],
-        [VMEM((16, LB, 128), F32)],
-    )(at, powers, pack_other)
+    load_call = call(load_kernel, [((CH, width), BF16, True)], [hbm], [pltpu.SemaphoreType.DMA((1,))], 4)
+    (value_near,) = load_call(value_weight)
     (out,) = call(
         last_kernel,
-        [((HROWS, width), BF16, False)],
-        [smem] + [True] * 7 + [hbm] * 6,
+        [((HROWS, width), BF16, None)],
+        [True] * 6 + [hbm] * 5,
         [
-            VMEM((4, LB, 128), F32), VMEM((2, HROWS, CH), BF16), VMEM((4, CH, width), BF16),
+            VMEM((4, LB, 128), F32), VMEM((2, HROWS, CH), BF16), VMEM((HROWS, width), BF16),
+            VMEM((3, CH, width), BF16),
             VMEM((1, width), F32), VMEM((1, width), F32),
-            pltpu.SemaphoreType.DMA((4 * (width // CHUNK) + 2,)),
+            VMEM((2, HROWS, FLAT), BF16), VMEM((2, HROWS, FLAT), BF16), VMEM((2, 4, LB, 128), F32),
+            VMEM((16, LB, 128), F32), pltpu.SemaphoreType.DMA((4 * (width // CHUNK) + 2,)),
         ],
         24,
     )(
-        at, planes, keep, mine, pack_other, *prepared, value_weight, gate_weight, value_other, gate_other,
+        planes, keep, mine, pack_other, powers, value_near, gate_weight, value_other, gate_other,
         value_bias.reshape(1, width), gate_bias.reshape(1, width),
     )
     return out

time: 59.4 us -> 57.2 us (0.963)
  Pallas kernels: 16.9 us -> 15 us
    pallas_call x5, Pallas kernels: 16.9 us -> 15 us  [run(): return fn(*placed)]
  transfers between devices with their start and end apart: 5 -> 5, of which waited for: 2 -> 2; matrix products, arithmetic and copies ran while one was open for 0% -> 0% of each run, Pallas kernels for 18% -> 19%
where the time goes in v3:
time: 57.2 us; the launch traced here: 56.8 us
  starting transfers between devices  30.2 us (53%)
  Pallas kernels  15 us (26%)
  waiting for transfers between devices  11.4 us (20%)
    all_to_all x2, starting transfers between devices, to_all(): return lax.all_to_all(copies, axes, split_axis=0, concat_axis=0, tiled=True)  16.9 us
    pallas_call x5, Pallas kernels, run(): return fn(*placed)  15 us
    all_to_all x2, waiting for transfers between devices, to_all(): return lax.all_to_all(copies, axes, split_axis=0, concat_axis=0, tiled=True)  11.4 us
    ppermute x1, starting transfers between devices, mixer(): value_other = lax.ppermute(value_weight, 'tp', SWAP)  8.74 us
    ppermute x1, starting transfers between devices, mixer(): pack_other = lax.ppermute(pack, 'tp', SWAP)  2.67 us
    ppermute x1, starting transfers between devices, mixer(): gate_other = lax.ppermute(gate_weight, 'tp', SWAP)  1.92 us
  transfers between devices with their start and end apart: 5, of which 2 were waited for; matrix products, arithmetic and copies ran while one was open for 0% of the time, Pallas kernels for 19%

profile of v3, /device:TPU:1, one launch (start us, length us, event | category | flops | bytes accessed | tf_op | source)
XLA Modules:
  0.0 56.8 jit_solution(10855154065421042611)
XLA Ops:
  0.0 8.7 %collective-permute-start.1 = (bf16[512,2048]{1,0:T(8,128)(2,1)}, bf16[512,2048]{1,0:T(8,128)(2,1)}, u32[]{:S(2)}, u32[]{:S(2)}) collective-permute-start(bf16[512,2048]{1,0:T(8,128)(2,1)} %w_hbm.1), channel_id=1, source_target_pairs={{0,1},{1,0},{2,3},{3,2},{4,5},{5,4},{6,7},{7,6},{8,9},{9,8},{10,11... | collective-permute-start | bytes 6291464 | tf_op jit(solution)/shard_map/ppermute | solution.py:464
  8.7 1.9 %collective-permute-start.2 = (bf16[512,2048]{1,0:T(8,128)(2,1)}, bf16[512,2048]{1,0:T(8,128)(2,1)}, u32[]{:S(2)}, u32[]{:S(2)}) collective-permute-start(bf16[512,2048]{1,0:T(8,128)(2,1)} %gw_hbm.1), channel_id=1, source_target_pairs={{0,1},{1,0},{2,3},{3,2},{4,5},{5,4},{6,7},{7,6},{8,9},{9,8},{10,11... | collective-permute-start | bytes 6291464 | tf_op jit(solution)/shard_map/ppermute | solution.py:465
  10.7 3.5 %shard_map.127 = (bf16[32,32,128]{2,1,0:T(8,128)(2,1)}, f32[4,16,128]{2,1,0:T(8,128)S(1)}, f32[2,8,2048]{2,1,0:T(8,128)S(1)}) custom-call(f32[32]{0:T(128)} %ls_hbm.3, f32[32,64]{1,0:T(8,128)} %lr_hbm.3, f32[32,64]{1,0:T(8,128)} %li_hbm.3, bf16[256,512]{1,0:T(8,128)(2,1)} %u_hbm.3, f32[512,64]{1,0:T(8,128)} %bitcast.11, f32[512,64]{1,0:T(8,128)} %bitcast.13), custom_call_target="tpu_custom_call" | custom-call | tf_op jit(solution)/shard_map/pallas_call | solution.py:415
  14.2 4.3 %all-to-all-start = ((bf16[32,32,128]{2,1,0:T(8,128)(2,1)}), bf16[32,32,128]{2,1,0:T(8,128)(2,1)S(1)}, u32[]{:S(2)}, u32[]{:S(2)}) async-start(bf16[32,32,128]{2,1,0:T(8,128)(2,1)} %get-tuple-element.11), calls=%async_computation | async-start | bytes 524288 | tf_op jit(solution)/shard_map/all_to_all | solution.py:421
  18.5 4.7 %shard_map.129 = (f32[128,512]{1,0:T(8,128)S(1)}, f32[512,128]{1,0:T(8,128)S(1)}, f32[1088,128]{1,0:T(8,128)}) custom-call(f32[32]{0:T(128)} %ls_hbm.3, f32[32,64]{1,0:T(8,128)} %lr_hbm.3, f32[32,64]{1,0:T(8,128)} %li_hbm.3, f32[512,64]{1,0:T(8,128)} %bitcast.15, f32[512,64]{1,0:T(8,128)} %bitcast.16, bf16[256,512]{1,0:T(8,128)(2,1)} %u_hbm.3, ...), custom_call_target="tpu_custom_call" | custom-call | tf_op jit(solution)/shard_map/pallas_call | solution.py:415
  23.2 2.7 %collective-permute-start = (f32[1088,128]{1,0:T(8,128)}, f32[1088,128]{1,0:T(8,128)S(1)}, u32[]{:S(2)}, u32[]{:S(2)}) collective-permute-start(f32[1088,128]{1,0:T(8,128)} %get-tuple-element.16), channel_id=1, source_target_pairs={{0,1},{1,0},{2,3},{3,2},{4,5},{5,4},{6,7},{7,6},{8,9},{9,8},{10,11... | collective-permute-start | bytes 1671176 | tf_op jit(solution)/shard_map/ppermute | solution.py:466
  25.9 4.2 %all-to-all-done.parts_ref = bf16[32,32,128]{2,1,0:T(8,128)(2,1)S(1)} async-done(((bf16[32,32,128]{2,1,0:T(8,128)(2,1)}), bf16[32,32,128]{2,1,0:T(8,128)(2,1)S(1)}, u32[]{:S(2)}, u32[]{:S(2)}) %all-to-all-start) | async-done | bytes 262176 | tf_op jit(solution)/shard_map/all_to_all | solution.py:421
  30.1 0.8 %shard_map.128 = bf16[16,32,128]{2,1,0:T(8,128)(2,1)} custom-call(bf16[32,32,128]{2,1,0:T(8,128)(2,1)S(1)} %all-to-all-done.parts_ref, f32[4,16,128]{2,1,0:T(8,128)S(1)} %get-tuple-element.12.a_ref.powers_ref), custom_call_target="tpu_custom_call" | custom-call | tf_op jit(solution)/shard_map/pallas_call | solution.py:415
  30.9 12.6 %all-to-all-start.1 = ((bf16[16,32,128]{2,1,0:T(8,128)(2,1)}), bf16[16,32,128]{2,1,0:T(8,128)(2,1)S(1)}, u32[]{:S(2)}, u32[]{:S(2)}) async-start(bf16[16,32,128]{2,1,0:T(8,128)(2,1)} %shard_map.128), calls=%async_computation.1 | async-start | bytes 262144 | tf_op jit(solution)/shard_map/all_to_all | solution.py:421
  43.4 1.6 %shard_map.130.vw_ref = bf16[512,2048]{1,0:T(8,128)(2,1)S(1)} custom-call(bf16[512,2048]{1,0:T(8,128)(2,1)} %w_hbm.1), custom_call_target="tpu_custom_call" | custom-call | tf_op jit(solution)/shard_map/pallas_call | solution.py:415
  45.0 0.0 collective-permute-done.other_ref
  45.0 7.3 %all-to-all-done.1.parts_ref = bf16[16,32,128]{2,1,0:T(8,128)(2,1)S(1)} async-done(((bf16[16,32,128]{2,1,0:T(8,128)(2,1)}), bf16[16,32,128]{2,1,0:T(8,128)(2,1)S(1)}, u32[]{:S(2)}, u32[]{:S(2)}) %all-to-all-start.1) | async-done | bytes 131104 | tf_op jit(solution)/shard_map/all_to_all | solution.py:421
  52.3 0.0 collective-permute-done.1.vo_hbm
  52.3 0.0 collective-permute-done.2.go_hbm
  52.3 4.5 %shard_map.131 = bf16[128,2048]{1,0:T(8,128)(2,1)} custom-call(bf16[16,32,128]{2,1,0:T(8,128)(2,1)S(1)} %all-to-all-done.1.parts_ref, f32[128,512]{1,0:T(8,128)S(1)} %get-tuple-element.14.keep_ref, f32[512,128]{1,0:T(8,128)S(1)} %get-tuple-element.15.mine_ref, f32[1088,128]{1,0:T(8,128)S(1)} %collective-permute-done.other_ref, ...), custom_call_target="tpu_custom_call" | custom-call | tf_op jit(solution)/shard_map/pallas_call | solution.py:415
Async XLA Ops:
  0.0 52.3 %collective-permute-start.1 = (bf16[512,2048]{1,0:T(8,128)(2,1)}, bf16[512,2048]{1,0:T(8,128)(2,1)}, u32[]{:S(2)}, u32[]{:S(2)}) collective-permute-start(bf16[512,2048]{1,0:T(8,128)(2,1)} %w_hbm.1), channel_id=1, source_target_pairs={{0,1},{1,0},{2,3},{3,2},{4,5},{5,4},{6,7},{7,6},{8,9},{9,8},{10,11... | collective-permute-start | bytes 6291464 | tf_op jit(solution)/shard_map/ppermute | solution.py:464
  8.7 43.6 %collective-permute-start.2 = (bf16[512,2048]{1,0:T(8,128)(2,1)}, bf16[512,2048]{1,0:T(8,128)(2,1)}, u32[]{:S(2)}, u32[]{:S(2)}) collective-permute-start(bf16[512,2048]{1,0:T(8,128)(2,1)} %gw_hbm.1), channel_id=1, source_target_pairs={{0,1},{1,0},{2,3},{3,2},{4,5},{5,4},{6,7},{7,6},{8,9},{9,8},{10,11... | collective-permute-start | bytes 6291464 | tf_op jit(solution)/shard_map/ppermute | solution.py:465
  14.2 15.9 %all-to-all-start = ((bf16[32,32,128]{2,1,0:T(8,128)(2,1)}), bf16[32,32,128]{2,1,0:T(8,128)(2,1)S(1)}, u32[]{:S(2)}, u32[]{:S(2)}) async-start(bf16[32,32,128]{2,1,0:T(8,128)(2,1)} %get-tuple-element.11), calls=%async_computation | async-start | bytes 524288 | tf_op jit(solution)/shard_map/all_to_all | solution.py:421
  23.2 21.8 %collective-permute-start = (f32[1088,128]{1,0:T(8,128)}, f32[1088,128]{1,0:T(8,128)S(1)}, u32[]{:S(2)}, u32[]{:S(2)}) collective-permute-start(f32[1088,128]{1,0:T(8,128)} %get-tuple-element.16), channel_id=1, source_target_pairs={{0,1},{1,0},{2,3},{3,2},{4,5},{5,4},{6,7},{7,6},{8,9},{9,8},{10,11... | collective-permute-start | bytes 1671176 | tf_op jit(solution)/shard_map/ppermute | solution.py:466
  30.9 21.5 %all-to-all-start.1 = ((bf16[16,32,128]{2,1,0:T(8,128)(2,1)}), bf16[16,32,128]{2,1,0:T(8,128)(2,1)S(1)}, u32[]{:S(2)}, u32[]{:S(2)}) async-start(bf16[16,32,128]{2,1,0:T(8,128)(2,1)} %shard_map.128), calls=%async_computation.1 | async-start | bytes 262144 | tf_op jit(solution)/shard_map/all_to_all | solution.py:421
